TPU v7x, 32 devices: a whole 2x2x4 slice. The times are simulated.
32 devices in a mesh: sp: 8 (over z, y), dp: 4 (over x, core).
Axes of the slice: x: 2, y: 2, z: 4, core: 2. Of those that a mesh axis runs over, the one named last changes fastest.
Arguments:
- inputs: bfloat16 [4, 1536, 2048], P('dp', 'sp'), may hold values from -6 to 6
- in_gain: float32 [2048], replicated, may hold values from 0.1 to 1.9
- w_query: bfloat16 [2048, 1024], P('dp', 'sp'), may hold values from -0.125 to 0.125
- w_key: bfloat16 [2048, 256], P('dp', 'sp'), may hold values from -0.375 to 0.375
- w_value: bfloat16 [2048, 256], P('dp', 'sp'), may hold values from -0.125 to 0.125
- key_bias: float32 [4, 1536, 16], P('dp', None, 'sp'), may hold values from -20 to 0
- out_gain: float32 [1024], replicated, may hold values from 0.1 to 1.9
- w_out: bfloat16 [1024, 2048], P('sp', 'dp'), may hold values from -0.1875 to 0.1875
Outputs:
- mixed: bfloat16 [4, 1536, 2048], P('dp', 'sp')
All inputs are finite; a program needn't handle non-finite values.
Results may differ from a plain program's by a relative error of at most 0.012.
The roundings to bfloat16 on the way count: a program that leaves them out, or rounds other values in their place, can miss the bound.
Values may be sent and summed in bfloat16 or wider, within the bound.
A program may use at most 128 MiB of HBM per device.

v0:
```python
import jax
import jax.numpy as jnp
from jax import lax
from jax.sharding import PartitionSpec as P

HEAD_DIM = 64


norm_eps = 1e-06


def from_partner(value, axis, distance):
    return lax.ppermute(value, axis, [(i, i ^ 1 << distance) for i in range(lax.axis_size(axis))])


def body(inputs, in_gain, w_query, w_key, w_value, key_bias, out_gain, w_out):
    width_sp = lax.axis_size("sp")
    own_index = lax.axis_index("sp")
    wide = inputs[0].astype(jnp.float32)
    normed_rows = (
        wide * lax.rsqrt(jnp.mean(wide * wide, axis=-1, keepdims=True) + norm_eps) * in_gain
    ).astype(jnp.bfloat16)
    local_rows = normed_rows.shape[0]
    w_query, w_key, w_value, w_out = (
        lax.all_gather(w_query, "dp", axis=0, tiled=True),
        lax.all_gather(w_key, "dp", axis=0, tiled=True),
        lax.all_gather(w_value, "dp", axis=0, tiled=True),
        lax.all_gather(w_out, "dp", axis=1, tiled=True),
    )
    w_key, w_value = (
        lax.all_gather(w_key, "sp", axis=1, tiled=True),
        lax.all_gather(w_value, "sp", axis=1, tiled=True),
    )
    keys = jnp.dot(normed_rows, w_key, preferred_element_type=jnp.float32).astype(jnp.bfloat16)
    values = jnp.dot(normed_rows, w_value, preferred_element_type=jnp.float32).astype(jnp.bfloat16)
    queries = jnp.dot(
        normed_rows,
        lax.all_gather(w_query, "sp", axis=1, tiled=True),
        preferred_element_type=jnp.float32,
    ).astype(jnp.bfloat16)
    heads_here = key_bias.shape[2]
    kv_heads = keys.shape[1] // HEAD_DIM
    spread = width_sp // kv_heads
    query_slots = queries.reshape(local_rows, width_sp, heads_here * HEAD_DIM)
    key_slots = keys.reshape(local_rows, width_sp, HEAD_DIM // spread)
    value_slots = values.reshape(local_rows, width_sp, HEAD_DIM // spread)
    query_all, key_mine, value_mine = (
        lax.all_to_all(query_slots, "sp", split_axis=1, concat_axis=0, tiled=True),
        lax.all_to_all(key_slots, "sp", split_axis=1, concat_axis=0, tiled=True),
        lax.all_to_all(value_slots, "sp", split_axis=1, concat_axis=0, tiled=True),
    )
    for section in range(spread.bit_length() - 1):
        key_other, value_other = from_partner((key_mine, value_mine), "sp", section)
        upper = own_index // 2**section % 2 == 1
        key_mine = jnp.where(
            upper,
            jnp.concatenate([key_other, key_mine], axis=2),
            jnp.concatenate([key_mine, key_other], axis=2),
        )
        value_mine = jnp.where(
            upper,
            jnp.concatenate([value_other, value_mine], axis=2),
            jnp.concatenate([value_mine, value_other], axis=2),
        )
    keys_head = key_mine[:, 0, :]
    values_head = value_mine[:, 0, :]
    length_all = query_all.shape[0]
    queries_head = query_all.reshape(length_all, heads_here, HEAD_DIM)
    bias_here = key_bias[0].T
    block = min(512, length_all)
    pieces = []
    for index in range(length_all // block):
        start = index * block
        end = start + block
        logits = jnp.einsum(
            "thd,sd->hts",
            queries_head[start:end],
            keys_head[:end],
            preferred_element_type=jnp.float32,
        )
        logits = logits * HEAD_DIM ** (-0.5) + bias_here[:, None, :end]
        rows = start + jnp.arange(block, dtype=jnp.int32)[:, None]
        columns = jnp.arange(end, dtype=jnp.int32)[None, :]
        strict = (columns < rows)[None, :, :]
        log_keep = jnp.where(strict, jax.nn.log_sigmoid(-logits), jnp.float32(0.0))
        log_rest = lax.cumsum(log_keep, axis=2, reverse=True) - log_keep
        sticks = jnp.where(
            strict, jnp.exp(jax.nn.log_sigmoid(logits) + log_rest), jnp.float32(0.0)
        ).astype(jnp.bfloat16)
        pieces.append(
            jnp.einsum("hts,sd->thd", sticks, values_head[:end], preferred_element_type=jnp.float32)
        )
    attended = jnp.concatenate(pieces, axis=0)
    gains = lax.dynamic_slice_in_dim(
        out_gain, own_index * heads_here * HEAD_DIM, heads_here * HEAD_DIM, 0
    )
    scaled = attended * lax.rsqrt(jnp.mean(attended * attended, axis=-1, keepdims=True) + norm_eps)
    head_out = (
        (scaled * gains.reshape(heads_here, HEAD_DIM))
        .astype(jnp.bfloat16)
        .reshape(length_all, 1, heads_here * HEAD_DIM)
    )
    returned = lax.all_to_all(head_out, "sp", split_axis=0, concat_axis=1, tiled=True)
    returned = returned.reshape(local_rows, width_sp * heads_here * HEAD_DIM)
    mixed = jnp.dot(
        returned,
        lax.all_gather(w_out, "sp", axis=0, tiled=True),
        preferred_element_type=jnp.float32,
    )
    return mixed.astype(jnp.bfloat16)[None]


def solution(mesh):
    placed = (
        P("dp", "sp", None),
        P(),
        P("dp", "sp"),
        P("dp", "sp"),
        P("dp", "sp"),
        P("dp", None, "sp"),
        P(),
        P("sp", "dp"),
    )
    return jax.shard_map(
        body, mesh=mesh, in_specs=placed, out_specs=P("dp", "sp", None), check_vma=False
    )
```

profile of v0, /device:TPU:0, one launch (start us, length us, event | category | flops | bytes accessed | tf_op | source)
XLA Modules:
  0.0 333.5 jit_solution(653828741404333262)
XLA Ops:
  6.5 8.5 %all_gather.24 = bf16[2048,32]{0,1:T(8,128)(2,1)} all-gather(bf16[512,32]{0,1:T(8,128)(2,1)} %param.12), channel_id=1, replica_groups=mesh['sp'=8,'dp'=4] {'dp'}, dimensions={0}, use_global_device_ids=true | all-gather | bytes 163840 | tf_op jit(solution)/shard_map/all_gather | solution.py:27
  15.1 6.1 %all_gather.26 = bf16[2048,32]{0,1:T(8,128)(2,1)} all-gather(bf16[512,32]{0,1:T(8,128)(2,1)} %param.11), channel_id=1, replica_groups=mesh['sp'=8,'dp'=4] {'dp'}, dimensions={0}, use_global_device_ids=true | all-gather | bytes 163840 | tf_op jit(solution)/shard_map/all_gather | solution.py:26
  21.3 9.1 %all_gather.28 = bf16[2048,128]{1,0:T(8,128)(2,1)} all-gather(bf16[512,128]{1,0:T(8,128)(2,1)} %param.10), channel_id=1, replica_groups=mesh['sp'=8,'dp'=4] {'dp'}, dimensions={0}, use_global_device_ids=true | all-gather | bytes 655360 | tf_op jit(solution)/shard_map/all_gather | solution.py:25
  30.5 8.4 %all_gather.30 = bf16[128,2048]{1,0:T(8,128)(2,1)} all-gather(bf16[128,512]{1,0:T(8,128)(2,1)} %param.15), channel_id=1, replica_groups=mesh['sp'=8,'dp'=4] {'dp'}, dimensions={1}, use_global_device_ids=true | all-gather | bytes 655360 | tf_op jit(solution)/shard_map/all_gather | solution.py:28
  38.9 0.7 slice.85
  39.6 0.7 slice.79
  40.3 1.4 fusion.28
  41.7 0.6 iota_compare_fusion
  42.3 1.3 dynamic_slice.3
  43.6 12.3 %all-gather.5.cloned.1.call-done = bf16[2048,256]{0,1:T(8,128)(2,1)} async-done(((bf16[2048,32]{0,1:T(8,128)(2,1)}), bf16[2048,256]{0,1:T(8,128)(2,1)}) %all-gather.5.cloned.1.call-update) | async-done | bytes 1048592 | tf_op jit(solution)/shard_map/all_gather | solution.py:32
  55.9 1.7 convolution_convert_fusion.3
  57.6 0.8 copy.61
  58.4 3.4 %all-to-all-start = ((bf16[192,8,32]{0,2,1:T(8,128)(2,1)}), bf16[192,8,32]{0,2,1:T(8,128)(2,1)S(1)}, u32[]{:S(2)}, u32[]{:S(2)}) async-start(bf16[192,8,32]{0,2,1:T(8,128)(2,1)} %bitcast.2), calls=%async_computation | async-start | bytes 262144 | tf_op jit(solution)/shard_map/all_to_all | solution.py:50
  61.8 35.2 %all-gather.7.cloned.1.call-done = bf16[2048,256]{0,1:T(8,128)(2,1)} async-done(((bf16[2048,32]{0,1:T(8,128)(2,1)}), bf16[2048,256]{0,1:T(8,128)(2,1)}) %all-gather.7.cloned.1.call-update) | async-done | bytes 1048592 | tf_op jit(solution)/shard_map/all_gather | solution.py:31
  97.0 1.7 convolution_convert_fusion.2
  98.8 0.8 copy.63
  99.5 3.4 %all-to-all-start.1 = ((bf16[192,8,32]{0,2,1:T(8,128)(2,1)}), bf16[192,8,32]{0,2,1:T(8,128)(2,1)S(1)}, u32[]{:S(2)}, u32[]{:S(2)}) async-start(bf16[192,8,32]{0,2,1:T(8,128)(2,1)} %bitcast.7), calls=%async_computation.1 | async-start | bytes 262144 | tf_op jit(solution)/shard_map/all_to_all | solution.py:49
  102.9 69.5 %all-gather.9.cloned.1.call-done = bf16[2048,1024]{1,0:T(8,128)(2,1)} async-done(((bf16[2048,128]{1,0:T(8,128)(2,1)}), bf16[2048,1024]{1,0:T(8,128)(2,1)}) %all-gather.9.cloned.1.call-update) | async-done | bytes 4194320 | tf_op jit(solution)/shard_map/all_gather | solution.py:38
  172.5 3.2 fusion.31
  175.7 0.8 copy.97
  176.5 3.9 %all-to-all-start.2 = ((bf16[192,8,128]{2,0,1:T(8,128)(2,1)}), bf16[192,8,128]{2,0,1:T(8,128)(2,1)S(1)}, u32[]{:S(2)}, u32[]{:S(2)}) async-start(bf16[192,8,128]{2,0,1:T(8,128)(2,1)} %bitcast.149), calls=%async_computation.2 | async-start | bytes 786432 | tf_op jit(solution)/shard_map/all_to_all | solution.py:48
  181.1 2.0 collective-permute-start
  183.9 8.7 %collective-permute-done = bf16[1536,1,32]{0,2,1:T(8,128)(2,1)S(1)} collective-permute-done((bf16[1536,1,32]{0,2,1:T(8,128)(2,1)S(1)}, bf16[1536,1,32]{0,2,1:T(8,128)(2,1)S(1)}, u32[]{:S(2)}, u32[]{:S(2)}) %collective-permute-start) | collective-permute-done | bytes 98336 | tf_op jit(solution)/shard_map/ppermute | solution.py:13
  192.5 4.0 %collective-permute-done.1 = bf16[1536,1,32]{0,2,1:T(8,128)(2,1)S(1)} collective-permute-done((bf16[1536,1,32]{0,2,1:T(8,128)(2,1)S(1)}, bf16[1536,1,32]{0,2,1:T(8,128)(2,1)S(1)}, u32[]{:S(2)}, u32[]{:S(2)}) %collective-permute-start.1) | collective-permute-done | bytes 98336 | tf_op jit(solution)/shard_map/ppermute | solution.py:13
  196.6 0.7 maximum_select_fusion
  197.3 3.4 %all-to-all-done.2 = bf16[192,8,128]{2,0,1:T(8,128)(2,1)S(1)} async-done(((bf16[192,8,128]{2,0,1:T(8,128)(2,1)}), bf16[192,8,128]{2,0,1:T(8,128)(2,1)S(1)}, u32[]{:S(2)}, u32[]{:S(2)}) %all-to-all-start.2) | async-done | bytes 393248 | tf_op jit(solution)/shard_map/all_to_all | solution.py:48
  201.6 4.8 %fusion.15 = (f32[2,512,1024]{1,2,0:T(8,128)S(1)}, f32[1024,512,2]{1,0,2:T(8,128)}) fusion(f32[2,1024]{1,0:T(2,128)S(1)} %slice.85, pred[512,1024]{0,1:T(8,128)(4,1)S(1)} %iota_compare_fusion.1, bf16[1536,2,64]{0,2,1:T(8,128)(2,1)S(1)} %reshape.341, bf16[1536,1,64]{0,2,1:T(8,128)(2,1)S(1)} %get-tuple-element.12), kind=kOutput, calls=%fused_computation.23 | convolution fusion | flops 144703488 | bytes 9183232 | tf_op jit(solution)/shard_map/thd,sd->hts/dot_general | solution.py:75
  206.3 10.1 %fusion.16 = f32[2,512,8,128]{1,2,3,0:T(8,128)S(1)} fusion(f32[2,512,8,128]{1,3,2,0:T(8,128)S(1)} %bitcast.156), kind=kOutput, calls=%fused_computation.26 | output fusion | flops 133169152 | bytes 8388608 | tf_op jit(solution)/shard_map/reduce-window.2
  216.4 1.9 copy-done.1
  218.5 2.7 broadcast_add_fusion.1
  221.2 4.5 %copy.71 = f32[2,512,8,128]{1,3,2,0:T(8,128)} copy(f32[2,512,8,128]{1,2,3,0:T(8,128)S(1)} %broadcast_add_fusion.1) | data formatting | bytes 8388608 | tf_op jit(solution)/shard_map/reduce_window_sum | solution.py:86
  225.7 6.5 %fusion.8 = (f32[2,512,1536]{1,2,0:T(8,128)S(1)}, f32[1536,512,2]{1,0,2:T(8,128)}) fusion(f32[2,1536]{1,0:T(2,128)S(1)} %bitcast.174, pred[512,1536]{0,1:T(8,128)(4,1)S(1)} %iota_compare_fusion, bf16[1536,2,64]{0,2,1:T(8,128)(2,1)S(1)} %reshape.341, bf16[1536,32]{0,1:T(8,128)(2,1)S(1)} %concatenate.93, bf16[1536,32]{0,1:T(8,128)(2,1)S(1)} %bitcast.171, ...), kind=kOutput, calls=%fused_computation.12 | convolution fusion | flops 217939968 | bytes 13709313 | tf_op jit(solution)/shard_map/thd,sd->hts/dot_general | solution.py:75
  232.2 20.3 %fusion = f32[2,512,12,128]{1,2,3,0:T(8,128)S(1)} fusion(f32[2,512,12,128]{1,3,2,0:T(8,128)S(1)} %bitcast.153), kind=kOutput, calls=%fused_computation.4 | output fusion | flops 199753728 | bytes 12582912 | tf_op jit(solution)/shard_map/reduce-window.4
  252.6 3.2 copy-done
  256.0 4.5 %broadcast_add_fusion = f32[2,512,12,128]{1,2,3,0:T(8,128)S(1)} fusion(f32[2,512,12,128]{1,2,3,0:T(8,128)} %copy-done, f32[2,512,12]{1,2,0:T(8,128)S(1)} %slice.90), kind=kLoop, calls=%fused_computation.28 | loop fusion | flops 1572864 | bytes 12632064 | tf_op jit(solution)/shard_map/reduce_window_sum | solution.py:86
  260.4 6.3 %copy.76 = f32[2,512,12,128]{1,3,2,0:T(8,128)} copy(f32[2,512,12,128]{1,2,3,0:T(8,128)S(1)} %broadcast_add_fusion) | data formatting | bytes 12582912 | tf_op jit(solution)/shard_map/reduce_window_sum | solution.py:86
  266.7 3.0 fusion.25
  269.7 9.8 %fusion.26 = f32[2,512,4,128]{1,2,3,0:T(4,128)S(1)} fusion(f32[2,512,4,128]{1,3,2,0:T(8,128)S(1)} %bitcast.164), kind=kOutput, calls=%fused_computation.41 | output fusion | flops 66584576 | bytes 4194304 | tf_op jit(solution)/shard_map/reduce-window
  280.1 0.6 copy.68
  280.7 3.1 copy-done.4
  283.8 3.2 fusion.23
  287.4 7.0 %fusion.13 = bf16[2,512,1024]{1,2,0:T(8,128)(2,1)S(1)} fusion(f32[2,512,8,128]{1,3,2,0:T(8,128)S(1)} %copy-done.2, f32[1024,512,2]{1,0,2:T(8,128)S(1)} %copy-done.3, f32[2,1024]{1,0:T(2,128)S(1)} %copy-done.14, pred[512,1024]{0,1:T(8,128)(4,1)S(1)} %iota_compare_fusion.1), kind=kLoop, calls=%fused_computation.21 | loop fusion | flops 23068672 | bytes 11018240 | tf_op jit(solution)/shard_map/convert_element_type | solution.py:89
  295.0 10.1 %fusion.6 = bf16[2,512,1536]{1,2,0:T(8,128)(2,1)S(1)} fusion(f32[2,512,12,128]{1,3,2,0:T(8,128)S(1)} %bitcast.152, f32[1536,512,2]{1,0,2:T(8,128)S(1)} %bitcast.155, f32[2,1536]{1,0:T(2,128)S(1)} %bitcast.175, pred[512,1536]{0,1:T(8,128)(4,1)S(1)} %iota_compare_fusion), kind=kLoop, calls=%fused_computation.10 | loop fusion | flops 34603008 | bytes 16527360 | tf_op jit(solution)/shard_map/convert_element_type | solution.py:89
  305.1 0.6 fusion.38
  306.0 0.5 broadcast.121
  306.6 0.9 reduce
  307.8 13.9 %all_to_all.66 = bf16[8,2,12288]{2,1,0:T(2,128)(2,1)S(1)} all-to-all(bf16[8,2,12288]{2,1,0:T(2,128)(2,1)S(1)} %reshape.356), channel_id=1, replica_groups=mesh['sp'=8,'dp'=4] {'sp'}, dimensions={0} | all-to-all | bytes 786432 | tf_op jit(solution)/shard_map/all_to_all | solution.py:103
  322.5 4.1 %fusion.18 = bf16[1,192,2048]{2,1,0:T(8,128)(2,1)} fusion(bf16[1024,2048]{1,0:T(8,128)(2,1)} %all-gather.11.cloned.1.call-done, bf16[24,8,8,128]{3,2,1,0:T(8,128)(2,1)S(1)} %bitcast.167), kind=kOutput, calls=%fused_computation.31 | convolution fusion | flops 805699584 | bytes 5373952 | tf_op jit(solution)/shard_map/dot_general | solution.py:105
  (91 shorter events, 5.2 us)
Async XLA Ops:
  6.5 49.4 %copy-start.7 = (bf16[1,192,2048]{2,1,0:T(8,128)(2,1)S(1)}, bf16[1,192,2048]{2,1,0:T(8,128)(2,1)}, u32[]{:S(2)}) copy-start(bf16[1,192,2048]{2,1,0:T(8,128)(2,1)} %param.8) | copy-start | bytes 2359300
  6.5 49.4 %copy-start.18 = (f32[2048]{0:T(1024)S(1)}, f32[2048]{0:T(1024)}, u32[]{:S(2)}) copy-start(f32[2048]{0:T(1024)} %param.9) | copy-start | bytes 24580
  6.5 49.4 %all-gather.5.cloned.1.call-start = ((), (), s32[]{:S(2)}) async-start(), calls=%async_computation.4 | async-start | bytes 1179648 | tf_op jit(solution)/shard_map/all_gather | solution.py:32
  15.1 82.0 %all-gather.7.cloned.1.call-start = ((), (), s32[]{:S(2)}) async-start(), calls=%async_computation.5 | async-start | bytes 1179648 | tf_op jit(solution)/shard_map/all_gather | solution.py:31
  21.2 151.2 %all-gather.9.cloned.1.call-start = ((), (), s32[]{:S(2)}) async-start(), calls=%async_computation.6 | async-start | bytes 4718592 | tf_op jit(solution)/shard_map/all_gather | solution.py:38
  30.4 292.0 %all-gather.11.cloned.1.call-start = ((), (), s32[]{:S(2)}) async-start(), calls=%async_computation.7 | async-start | bytes 4718592 | tf_op jit(solution)/shard_map/all_gather | solution.py:107
  39.6 161.9 %copy-start.13 = (f32[2,1024]{1,0:T(2,128)}, f32[2,1024]{1,0:T(2,128)S(1)}, u32[]{:S(2)}) copy-start(f32[2,1024]{1,0:T(2,128)S(1)} %slice.85) | copy-start | bytes 24580
  40.3 226.4 %copy-start.15 = (f32[2,512]{1,0:T(2,128)}, f32[2,512]{1,0:T(2,128)S(1)}, u32[]{:S(2)}) copy-start(f32[2,512]{1,0:T(2,128)S(1)} %slice.79) | copy-start | bytes 12292
  58.4 41.1 %all-to-all-start = ((bf16[192,8,32]{0,2,1:T(8,128)(2,1)}), bf16[192,8,32]{0,2,1:T(8,128)(2,1)S(1)}, u32[]{:S(2)}, u32[]{:S(2)}) async-start(bf16[192,8,32]{0,2,1:T(8,128)(2,1)} %bitcast.2), calls=%async_computation | async-start | bytes 262144 | tf_op jit(solution)/shard_map/all_to_all | solution.py:50
  99.5 77.0 %all-to-all-start.1 = ((bf16[192,8,32]{0,2,1:T(8,128)(2,1)}), bf16[192,8,32]{0,2,1:T(8,128)(2,1)S(1)}, u32[]{:S(2)}, u32[]{:S(2)}) async-start(bf16[192,8,32]{0,2,1:T(8,128)(2,1)} %bitcast.7), calls=%async_computation.1 | async-start | bytes 262144 | tf_op jit(solution)/shard_map/all_to_all | solution.py:49
  176.5 24.2 %all-to-all-start.2 = ((bf16[192,8,128]{2,0,1:T(8,128)(2,1)}), bf16[192,8,128]{2,0,1:T(8,128)(2,1)S(1)}, u32[]{:S(2)}, u32[]{:S(2)}) async-start(bf16[192,8,128]{2,0,1:T(8,128)(2,1)} %bitcast.149), calls=%async_computation.2 | async-start | bytes 786432 | tf_op jit(solution)/shard_map/all_to_all | solution.py:48
  181.1 11.5 %collective-permute-start = (bf16[1536,1,32]{0,2,1:T(8,128)(2,1)S(1)}, bf16[1536,1,32]{0,2,1:T(8,128)(2,1)S(1)}, u32[]{:S(2)}, u32[]{:S(2)}) collective-permute-start(bf16[1536,1,32]{0,2,1:T(8,128)(2,1)S(1)} %all_to_all.51), channel_id=1, source_target_pairs={{0,4},{4,0},{8,12},{12,8},{16,20},{20,16},{24,28},{28,24},{1,5},{5... | collective-permute-start | bytes 294920 | tf_op jit(solution)/shard_map/ppermute | solution.py:13
  183.3 13.3 %collective-permute-start.1 = (bf16[1536,1,32]{0,2,1:T(8,128)(2,1)S(1)}, bf16[1536,1,32]{0,2,1:T(8,128)(2,1)S(1)}, u32[]{:S(2)}, u32[]{:S(2)}) collective-permute-start(bf16[1536,1,32]{0,2,1:T(8,128)(2,1)S(1)} %all_to_all.55), channel_id=1, source_target_pairs={{0,4},{4,0},{8,12},{12,8},{16,20},{20,16},{24,28},{28,24},{1,5},{5... | collective-permute-start | bytes 294920 | tf_op jit(solution)/shard_map/ppermute | solution.py:13
  183.6 83.2 %copy-start.5 = (pred[512,512]{0,1:T(8,128)(4,1)}, pred[512,512]{0,1:T(8,128)(4,1)S(1)}, u32[]{:S(2)}) copy-start(pred[512,512]{0,1:T(8,128)(4,1)S(1)} %iota_compare_fusion.2) | copy-start | bytes 786436
  192.5 13.8 %copy-start.9 = (bf16[1536,1,32]{0,2,1:T(8,128)(2,1)}, bf16[1536,1,32]{0,2,1:T(8,128)(2,1)S(1)}, u32[]{:S(2)}) copy-start(bf16[1536,1,32]{0,2,1:T(8,128)(2,1)S(1)} %collective-permute-done) | copy-start | bytes 294916
  216.4 1.9 copy-start.1
  221.2 4.5 %copy-start.11 = (f32[1,1536,2]{1,2,0:T(2,128)S(1)}, f32[1,1536,2]{1,2,0:T(2,128)}, u32[]{:S(2)}) copy-start(f32[1,1536,2]{1,2,0:T(2,128)} %param.13) | copy-start | bytes 36868
  252.6 3.2 copy-start
  279.7 4.2 %copy-start.4 = (f32[512,512,2]{1,0,2:T(8,128)S(1)}, f32[512,512,2]{1,0,2:T(8,128)}, u32[]{:S(2)}) copy-start(f32[512,512,2]{1,0,2:T(8,128)} %get-tuple-element.10) | copy-start | bytes 6291460
  279.7 4.1 %copy-start.6 = (pred[512,512]{0,1:T(8,128)(4,1)S(1)}, pred[512,512]{0,1:T(8,128)(4,1)}, u32[]{:S(2)}) copy-start(pred[512,512]{0,1:T(8,128)(4,1)} %copy-done.5) | copy-start | bytes 786436
  279.7 4.1 %copy-start.16 = (f32[2,512]{1,0:T(2,128)S(1)}, f32[2,512]{1,0:T(2,128)}, u32[]{:S(2)}) copy-start(f32[2,512]{1,0:T(2,128)} %copy-done.15) | copy-start | bytes 12292
  279.7 15.2 %slice-start.2 = ((s8[6291456]{0:T(1024)(128)(4,1)}), s8[4194304]{0:T(1024)(128)(4,1)S(1)}, s32[]{:S(2)}) async-start(s8[6291456]{0:T(1024)(128)(4,1)} %bitcast.154), calls=%async_computation.10 | async-start | bytes 8388608
  280.1 7.0 %copy-start.8 = (bf16[1536,1,64]{0,2,1:T(8,128)(2,1)S(1)}, bf16[1536,1,64]{0,2,1:T(8,128)(2,1)}, u32[]{:S(2)}) copy-start(bf16[1536,1,64]{0,2,1:T(8,128)(2,1)} %get-tuple-element.11) | copy-start | bytes 589828
  280.1 7.3 %copy-start.3 = (f32[1024,512,2]{1,0,2:T(8,128)S(1)}, f32[1024,512,2]{1,0,2:T(8,128)}, u32[]{:S(2)}) copy-start(f32[1024,512,2]{1,0,2:T(8,128)} %get-tuple-element.8) | copy-start | bytes 12582916
  280.7 6.7 %copy-start.2 = (f32[2,512,8,128]{1,3,2,0:T(8,128)S(1)}, f32[2,512,8,128]{1,3,2,0:T(8,128)}, u32[]{:S(2)}) copy-start(f32[2,512,8,128]{1,3,2,0:T(8,128)} %copy.71) | copy-start | bytes 12582916
  280.7 6.7 %copy-start.14 = (f32[2,1024]{1,0:T(2,128)S(1)}, f32[2,1024]{1,0:T(2,128)}, u32[]{:S(2)}) copy-start(f32[2,1024]{1,0:T(2,128)} %copy-done.13) | copy-start | bytes 24580
  287.1 7.8 %slice-start = ((s8[6291456]{0:T(1024)(128)(4,1)}), s8[4194304]{0:T(1024)(128)(4,1)S(1)}, s32[]{:S(2)}) async-start(s8[6291456]{0:T(1024)(128)(4,1)} %bitcast.151), calls=%async_computation.8 | async-start | bytes 8388608
  287.1 7.8 %slice-start.3 = ((s8[6291456]{0:T(1024)(128)(4,1)}), s8[2097152]{0:T(1024)(128)(4,1)S(1)}, s32[]{:S(2)}) async-start(s8[6291456]{0:T(1024)(128)(4,1)} %bitcast.154), calls=%async_computation.11 | async-start | bytes 4194304
  287.4 7.5 %slice-start.1 = ((s8[6291456]{0:T(1024)(128)(4,1)}), s8[2097152]{0:T(1024)(128)(4,1)S(1)}, s32[]{:S(2)}) async-start(s8[6291456]{0:T(1024)(128)(4,1)} %bitcast.151), calls=%async_computation.9 | async-start | bytes 4194304
  287.4 7.5 %copy-start.12 = (f32[1,1536,2]{1,2,0:T(2,128)S(1)}, f32[1,1536,2]{1,2,0:T(2,128)}, u32[]{:S(2)}) copy-start(f32[1,1536,2]{1,2,0:T(2,128)} %param.13) | copy-start | bytes 36868
  294.9 10.1 %copy-start.10 = (bf16[1536,1,32]{0,2,1:T(8,128)(2,1)S(1)}, bf16[1536,1,32]{0,2,1:T(8,128)(2,1)}, u32[]{:S(2)}) copy-start(bf16[1536,1,32]{0,2,1:T(8,128)(2,1)} %copy-done.9) | copy-start | bytes 294916
  305.0 0.9 copy-start.17
Sparse Core Ops, SparseCore 0:
  15.2 40.6 all-gather.4
  58.0 38.9 all-gather.6
  99.1 73.3 all-gather.8
  174.4 77.8 all-gather.10
where the time goes:
time: 338 us; the launch traced here: 333 us
  waiting for transfers between devices  133 us (39%)
  other arithmetic  72.6 us (21%)
  blocking collectives  46 us (14%)
  local copies, waits for them, and re-layouts  27.9 us (8%)
  matrix products  26.5 us (8%)
  between operations  14.2 us (4%)
  starting transfers between devices  12.9 us (4%)
    all_gather x1, waiting for transfers between devices, body(): lax.all_gather(w_query, 'sp', axis=1, tiled=True)  69.5 us
    another operation x6, other arithmetic  40.5 us
    all_gather x1, waiting for transfers between devices, body(): lax.all_gather(w_key, 'sp', axis=1, tiled=True)  35.2 us
    convert_element_type x3, other arithmetic, body(): sticks = jnp.where(strict, jnp.exp(jax.nn.log_sigmoid(logits) + log_rest)...  20.3 us
    dot_general x3, matrix products, body(): jnp.einsum('thd,sd->hts', queries_head[start:end], keys_head[:end], prefe...  14.3 us
    all_to_all x1, blocking collectives, body(): lax.all_to_all(head_out, 'sp', split_axis=0, concat_axis=1, tiled=True)  13.9 us
    ppermute x2, waiting for transfers between devices, from_partner(): lax.ppermute(value, axis, [(i, i ^ 1 << distance) for i in range(lax.axis...  12.7 us
    all_gather x1, waiting for transfers between devices, body(): lax.all_gather(w_value, 'sp', axis=1, tiled=True)  12.3 us
  transfers between devices with their start and end apart: 9, of which 6 were waited for; matrix products, arithmetic and copies ran while one was open for 34% of the time, Pallas kernels for 0%

commit v1 on v0

--- a/solution.py
+++ b/solution.py
@@ -1,6 +1,10 @@
+import functools
+
 import jax
 import jax.numpy as jnp
 from jax import lax
+from jax.experimental import pallas as pl
+from jax.experimental.pallas import tpu as pltpu
 from jax.sharding import PartitionSpec as P
 
 HEAD_DIM = 64
@@ -11,6 +15,86 @@
 
 def from_partner(value, axis, distance):
     return lax.ppermute(value, axis, [(i, i ^ 1 << distance) for i in range(lax.axis_size(axis))])
+
+
+def attention_kernel(block, q_ref, k_ref, v_ref, bias_ref, gain_ref, out_ref):
+    heads = bias_ref.shape[0]
+    index = pl.program_id(0)
+    row = lax.broadcasted_iota(jnp.int32, (block, block), 0)
+    column = lax.broadcasted_iota(jnp.int32, (block, block), 1)
+    later = jnp.where(row > column, 1.0, 0.0).astype(jnp.bfloat16)
+    strict = column < row
+    q_heads = [
+        q_ref[:, h * HEAD_DIM : (h + 1) * HEAD_DIM] * jnp.bfloat16(HEAD_DIM**-0.5)
+        for h in range(heads)
+    ]
+
+    def tile(j, h, rest, total, diagonal):
+        window = pl.ds(pl.multiple_of(j * block, block), block)
+        x = lax.dot_general(
+            q_heads[h], k_ref[window, :], (((1,), (1,)), ((), ())),
+            preferred_element_type=jnp.float32,
+        ) + bias_ref[h : h + 1, window]
+        soft = jnp.log(1.0 + jnp.exp(-jnp.abs(x)))
+        take = jnp.minimum(x, 0.0) - soft
+        keep = jnp.minimum(-x, 0.0) - soft
+        if diagonal:
+            keep = jnp.where(strict, keep, 0.0)
+        high = keep.astype(jnp.bfloat16)
+        low = (keep - high.astype(jnp.float32)).astype(jnp.bfloat16)
+        after = jnp.dot(high, later, preferred_element_type=jnp.float32) + jnp.dot(
+            low, later, preferred_element_type=jnp.float32
+        )
+        sticks = jnp.exp(take + (after + rest))
+        if diagonal:
+            sticks = jnp.where(strict, sticks, 0.0)
+        total = total + jnp.dot(
+            sticks.astype(jnp.bfloat16), v_ref[window, :], preferred_element_type=jnp.float32
+        )
+        return rest + (after[:, :1] + keep[:, :1]), total
+
+    state = []
+    for h in range(heads):
+        state += tile(
+            index, h, jnp.zeros((block, 1), jnp.float32),
+            jnp.zeros((block, HEAD_DIM), jnp.float32), True,
+        )
+
+    def step(n, state):
+        out = []
+        for h in range(heads):
+            out += tile(index - 1 - n, h, state[2 * h], state[2 * h + 1], False)
+        return tuple(out)
+
+    state = lax.fori_loop(0, index, step, tuple(state))
+    for h in range(heads):
+        total = state[2 * h + 1]
+        lanes = slice(h * HEAD_DIM, (h + 1) * HEAD_DIM)
+        scaled = total * lax.rsqrt(jnp.mean(total * total, axis=-1, keepdims=True) + norm_eps)
+        out_ref[:, lanes] = (scaled * gain_ref[:, lanes]).astype(jnp.bfloat16)
+
+
+def attention(q, k, v, bias, gains):
+    length, width = q.shape
+    block = min(256, length)
+    pairs = length * length // 2 * bias.shape[0]
+    return pl.pallas_call(
+        functools.partial(attention_kernel, block),
+        out_shape=jax.ShapeDtypeStruct((length, width), jnp.bfloat16),
+        grid=(length // block,),
+        in_specs=[
+            pl.BlockSpec((block, width), lambda i: (i, 0)),
+            pl.BlockSpec(k.shape, lambda i: (0, 0)),
+            pl.BlockSpec(v.shape, lambda i: (0, 0)),
+            pl.BlockSpec(bias.shape, lambda i: (0, 0)),
+            pl.BlockSpec(gains.shape, lambda i: (0, 0)),
+        ],
+        out_specs=pl.BlockSpec((block, width), lambda i: (i, 0)),
+        cost_estimate=pl.CostEstimate(
+            flops=pairs * 1500, bytes_accessed=length * width * 8, transcendentals=pairs * 3
+        ),
+        name="attention",
+    )(q, k, v, bias, gains)
 
 
 def body(inputs, in_gain, w_query, w_key, w_value, key_bias, out_gain, w_out):
@@ -65,41 +149,17 @@
     keys_head = key_mine[:, 0, :]
     values_head = value_mine[:, 0, :]
     length_all = query_all.shape[0]
-    queries_head = query_all.reshape(length_all, heads_here, HEAD_DIM)
-    bias_here = key_bias[0].T
-    block = min(512, length_all)
-    pieces = []
-    for index in range(length_all // block):
-        start = index * block
-        end = start + block
-        logits = jnp.einsum(
-            "thd,sd->hts",
-            queries_head[start:end],
-            keys_head[:end],
-            preferred_element_type=jnp.float32,
-        )
-        logits = logits * HEAD_DIM ** (-0.5) + bias_here[:, None, :end]
-        rows = start + jnp.arange(block, dtype=jnp.int32)[:, None]
-        columns = jnp.arange(end, dtype=jnp.int32)[None, :]
-        strict = (columns < rows)[None, :, :]
-        log_keep = jnp.where(strict, jax.nn.log_sigmoid(-logits), jnp.float32(0.0))
-        log_rest = lax.cumsum(log_keep, axis=2, reverse=True) - log_keep
-        sticks = jnp.where(
-            strict, jnp.exp(jax.nn.log_sigmoid(logits) + log_rest), jnp.float32(0.0)
-        ).astype(jnp.bfloat16)
-        pieces.append(
-            jnp.einsum("hts,sd->thd", sticks, values_head[:end], preferred_element_type=jnp.float32)
-        )
-    attended = jnp.concatenate(pieces, axis=0)
     gains = lax.dynamic_slice_in_dim(
         out_gain, own_index * heads_here * HEAD_DIM, heads_here * HEAD_DIM, 0
+    ).reshape(1, heads_here * HEAD_DIM)
+    head_out = attention(
+        query_all.reshape(length_all, heads_here * HEAD_DIM),
+        keys_head,
+        values_head,
+        key_bias[0].T,
+        gains,
     )
-    scaled = attended * lax.rsqrt(jnp.mean(attended * attended, axis=-1, keepdims=True) + norm_eps)
-    head_out = (
-        (scaled * gains.reshape(heads_here, HEAD_DIM))
-        .astype(jnp.bfloat16)
-        .reshape(length_all, 1, heads_here * HEAD_DIM)
-    )
+    head_out = head_out.reshape(length_all, 1, heads_here * HEAD_DIM)
     returned = lax.all_to_all(head_out, "sp", split_axis=0, concat_axis=1, tiled=True)
     returned = returned.reshape(local_rows, width_sp * heads_here * HEAD_DIM)
     mixed = jnp.dot(

time: 338 us -> 272 us (0.80); the launches traced: 333 us -> 272 us
  other arithmetic: 72.6 us -> 4.55 us
  Pallas kernels: 0 us -> 26.5 us
  local copies, waits for them, and re-layouts: 27.9 us -> 5.42 us
  matrix products: 26.5 us -> 10.8 us
  waiting for transfers between devices: 133 us -> 147 us
  blocking collectives: 46 us -> 51.7 us
    another operation x9 -> x0, other arithmetic: 48 us -> none
    pallas_call x0 -> x1, Pallas kernels: none -> 26.5 us  [attention(): pl.pallas_call(functools.partial(attention_kernel, block), out_shape=jax....]
    all_gather x1, waiting for transfers between devices: 12.3 us -> 35.2 us  [body(): lax.all_gather(w_value, 'sp', axis=1, tiled=True)]
    convert_element_type x5 -> x0, other arithmetic: 21.3 us -> none  [the longest x3 20.3 us: body(): sticks = jnp.where(strict, jnp.exp(jax.nn.log_sigmoid(logits) + log_rest)...]
    all_gather x1, waiting for transfers between devices: 35.2 us -> 17.4 us  [body(): lax.all_gather(w_key, 'sp', axis=1, tiled=True)]
    dot_general x6 -> x0, matrix products: 15.7 us -> none  [the longest x3 14.3 us: body(): jnp.einsum('thd,sd->hts', queries_head[start:end], keys_head[:end], prefe...]
    ppermute x2, waiting for transfers between devices: 12.7 us -> 24.6 us  [from_partner(): lax.ppermute(value, axis, [(i, i ^ 1 << distance) for i in range(lax.axis...]
    another operation x9 -> x0, local copies, waits for them, and re-layouts: 11.5 us -> none  [the longest x3 11.4 us: body(): log_rest = lax.cumsum(log_keep, axis=2, reverse=True) - log_keep]
  transfers between devices with their start and end apart: 9 -> 9, of which waited for: 6 -> 5; matrix products, arithmetic and copies ran while one was open for 34% -> 6% of each run, Pallas kernels for 0% -> 10%
where the time goes in v1:
time: 272 us
  waiting for transfers between devices  147 us (54%)
  blocking collectives  51.7 us (19%)
  Pallas kernels  26.5 us (10%)
  between operations  13.3 us (5%)
  starting transfers between devices  12.5 us (5%)
  matrix products  10.8 us (4%)
  local copies, waits for them, and re-layouts  5.42 us (2%)
  other arithmetic  4.55 us (2%)
    all_gather x1, waiting for transfers between devices, body(): lax.all_gather(w_query, 'sp', axis=1, tiled=True)  69.5 us
    all_gather x1, waiting for transfers between devices, body(): lax.all_gather(w_value, 'sp', axis=1, tiled=True)  35.2 us
    pallas_call x1, Pallas kernels, attention(): pl.pallas_call(functools.partial(attention_kernel, block), out_shape=jax....  26.5 us
    ppermute x2, waiting for transfers between devices, from_partner(): lax.ppermute(value, axis, [(i, i ^ 1 << distance) for i in range(lax.axis...  24.6 us
    all_to_all x1, blocking collectives, body(): lax.all_to_all(head_out, 'sp', split_axis=0, concat_axis=1, tiled=True)  20.3 us
    all_gather x1, waiting for transfers between devices, body(): lax.all_gather(w_key, 'sp', axis=1, tiled=True)  17.4 us
    all_gather x1, blocking collectives, body(): lax.all_gather(w_query, 'dp', axis=0, tiled=True)  9.1 us
    all_gather x1, blocking collectives, body(): lax.all_gather(w_key, 'dp', axis=0, tiled=True)  8.52 us
  transfers between devices with their start and end apart: 9, of which 5 were waited for; matrix products, arithmetic and copies ran while one was open for 6% of the time, Pallas kernels for 10%

profile of v1, /device:TPU:0, one launch (start us, length us, event | category | flops | bytes accessed | tf_op | source)
XLA Modules:
  0.0 271.6 jit_solution(17660254344922302956)
XLA Ops:
  6.5 8.5 %all_gather.26 = bf16[2048,32]{0,1:T(8,128)(2,1)} all-gather(bf16[512,32]{0,1:T(8,128)(2,1)} %param.11), channel_id=1, replica_groups=mesh['sp'=8,'dp'=4] {'dp'}, dimensions={0}, use_global_device_ids=true | all-gather | bytes 163840 | tf_op jit(solution)/shard_map/all_gather | solution.py:110
  15.1 0.0 all-gather.7.cloned.1.call-update
  15.1 0.0 all-gather.9.cloned.1.call-start
  15.1 6.1 %all_gather.28 = bf16[2048,32]{0,1:T(8,128)(2,1)} all-gather(bf16[512,32]{0,1:T(8,128)(2,1)} %param.12), channel_id=1, replica_groups=mesh['sp'=8,'dp'=4] {'dp'}, dimensions={0}, use_global_device_ids=true | all-gather | bytes 163840 | tf_op jit(solution)/shard_map/all_gather | solution.py:111
  21.2 0.0 all-gather.9.cloned.1.call-update
  21.2 0.0 copy-start.4
  21.3 0.0 all-gather.5.cloned.1.call-start
  21.3 9.1 %all_gather.24 = bf16[2048,128]{1,0:T(8,128)(2,1)} all-gather(bf16[512,128]{1,0:T(8,128)(2,1)} %param.10), channel_id=1, replica_groups=mesh['sp'=8,'dp'=4] {'dp'}, dimensions={0}, use_global_device_ids=true | all-gather | bytes 655360 | tf_op jit(solution)/shard_map/all_gather | solution.py:109
  30.4 0.0 all-gather.5.cloned.1.call-update
  30.4 0.0 all-gather.11.cloned.1.call-start
  30.5 7.7 %all_gather.30 = bf16[128,2048]{1,0:T(8,128)(2,1)} all-gather(bf16[128,512]{1,0:T(8,128)(2,1)S(1)} %copy-done.3), channel_id=1, replica_groups=mesh['sp'=8,'dp'=4] {'dp'}, dimensions={1}, use_global_device_ids=true | all-gather | bytes 655360 | tf_op jit(solution)/shard_map/all_gather | solution.py:112
  38.2 0.0 all-gather.11.cloned.1.call-update
  38.3 0.2 fusion.1
  38.5 17.4 %all-gather.7.cloned.1.call-done = bf16[2048,256]{0,1:T(8,128)(2,1)} async-done(((bf16[2048,32]{0,1:T(8,128)(2,1)}), bf16[2048,256]{0,1:T(8,128)(2,1)}) %all-gather.7.cloned.1.call-update) | async-done | bytes 1048592 | tf_op jit(solution)/shard_map/all_gather | solution.py:115
  55.9 1.8 convolution_convert_fusion.3
  57.7 0.8 copy.30
  58.4 3.4 %all-to-all-start.1 = ((bf16[192,8,32]{0,2,1:T(8,128)(2,1)}), bf16[192,8,32]{0,2,1:T(8,128)(2,1)S(1)}, u32[]{:S(2)}, u32[]{:S(2)}) async-start(bf16[192,8,32]{0,2,1:T(8,128)(2,1)} %bitcast.5), calls=%async_computation.1 | async-start | bytes 262144 | tf_op jit(solution)/shard_map/all_to_all | solution.py:133
  61.8 35.2 %all-gather.9.cloned.1.call-done = bf16[2048,256]{0,1:T(8,128)(2,1)} async-done(((bf16[2048,32]{0,1:T(8,128)(2,1)}), bf16[2048,256]{0,1:T(8,128)(2,1)}) %all-gather.9.cloned.1.call-update) | async-done | bytes 1048592 | tf_op jit(solution)/shard_map/all_gather | solution.py:116
  97.1 1.8 convolution_convert_fusion.2
  98.8 0.8 copy.33
  99.6 0.0 all-to-all-done.1
  99.6 3.4 %all-to-all-start.2 = ((bf16[192,8,32]{0,2,1:T(8,128)(2,1)}), bf16[192,8,32]{0,2,1:T(8,128)(2,1)S(1)}, u32[]{:S(2)}, u32[]{:S(2)}) async-start(bf16[192,8,32]{0,2,1:T(8,128)(2,1)} %bitcast.12), calls=%async_computation.2 | async-start | bytes 262144 | tf_op jit(solution)/shard_map/all_to_all | solution.py:134
  103.0 69.5 %all-gather.5.cloned.1.call-done = bf16[2048,1024]{1,0:T(8,128)(2,1)} async-done(((bf16[2048,128]{1,0:T(8,128)(2,1)}), bf16[2048,1024]{1,0:T(8,128)(2,1)}) %all-gather.5.cloned.1.call-update) | async-done | bytes 4194320 | tf_op jit(solution)/shard_map/all_gather | solution.py:122
  172.5 3.2 %fusion.4 = bf16[24,8,8,128]{3,2,1,0:T(8,128)(2,1)S(1)} fusion(bf16[2048,1024]{1,0:T(8,128)(2,1)} %all-gather.5.cloned.1.call-done, bf16[1,192,2048]{2,1,0:T(8,128)(2,1)S(1)} %copy-done.1, f32[2048]{0:T(1024)S(1)} %copy-done.4, f32[192]{0:T(256)S(1)} %add_rsqrt_fusion), kind=kOutput, calls=%fused_computation.8 | convolution fusion | flops 807075840 | bytes 5382912 | tf_op jit(solution)/shard_map/dot_general | solution.py:120
  175.7 0.8 copy.46
  176.6 0.0 all-to-all-done.2
  176.6 3.5 %all-to-all-start = ((bf16[192,8,128]{2,0,1:T(8,128)(2,1)}), bf16[192,8,128]{2,0,1:T(8,128)(2,1)S(1)}, u32[]{:S(2)}, u32[]{:S(2)}) async-start(bf16[192,8,128]{2,0,1:T(8,128)(2,1)} %bitcast.51), calls=%async_computation | async-start | bytes 786432 | tf_op jit(solution)/shard_map/all_to_all | solution.py:132
  180.0 0.2 copy.31
  180.3 2.0 collective-permute-start
  182.2 0.6 dynamic-slice_bitcast_fusion.gain_ref
  182.8 0.2 copy.34
  183.1 0.2 collective-permute-start.1
  183.2 18.4 %collective-permute-done = bf16[1536,1,32]{2,0,1:T(8,128)(2,1)S(1)} collective-permute-done((bf16[1536,1,32]{2,0,1:T(8,128)(2,1)S(1)}, bf16[1536,1,32]{2,0,1:T(8,128)(2,1)S(1)}, u32[]{:S(2)}, u32[]{:S(2)}) %collective-permute-start) | collective-permute-done | bytes 98336 | tf_op jit(solution)/shard_map/ppermute | solution.py:17
  201.6 1.2 maximum_select_fusion.k_ref
  202.8 6.3 %collective-permute-done.1 = bf16[1536,1,32]{2,0,1:T(8,128)(2,1)S(1)} collective-permute-done((bf16[1536,1,32]{2,0,1:T(8,128)(2,1)S(1)}, bf16[1536,1,32]{2,0,1:T(8,128)(2,1)S(1)}, u32[]{:S(2)}, u32[]{:S(2)}) %collective-permute-start.1) | collective-permute-done | bytes 98336 | tf_op jit(solution)/shard_map/ppermute | solution.py:17
  209.0 1.2 maximum_select_fusion.1.v_ref
  210.2 0.0 all-to-all-done
  210.2 0.7 copy-done.2
  211.0 26.5 %attention.1 = bf16[1536,128]{1,0:T(8,128)(2,1)} custom-call(bf16[1536,128]{1,0:T(8,128)(2,1)} %bitcast.60, bf16[1536,64]{1,0:T(8,128)(2,1)} %maximum_select_fusion.k_ref, bf16[1536,64]{1,0:T(8,128)(2,1)} %maximum_select_fusion.1.v_ref, f32[2,1536]{1,0:T(2,128)} %bitcast.64, f32[1,128]{1,0:T(1,128)} %dynamic-slice_bitcast_fusion.gain_ref), custom_call_target="tpu_custom_call" | custom-call | flops 3538944000 | bytes 1572864 | tf_op jit(solution)/shard_map/attention/pallas_call | solution.py:81
  237.5 0.5 broadcast.20
  238.0 1.9 reduce
  239.9 0.1 reshape.88
  240.0 20.3 %all_to_all.66 = bf16[8,2,12288]{2,1,0:T(2,128)(2,1)S(1)} all-to-all(bf16[8,2,12288]{2,1,0:T(2,128)(2,1)S(1)} %reshape.88), channel_id=1, replica_groups=mesh['sp'=8,'dp'=4] {'sp'}, dimensions={0} | all-to-all | bytes 786432 | tf_op jit(solution)/shard_map/all_to_all | solution.py:163
  260.3 0.4 reshape.89
  260.7 0.1 copy.38
  260.8 0.3 copy.37
  261.0 0.0 all-gather.11.cloned.1.call-done
  261.1 4.1 %fusion = bf16[1,192,2048]{2,1,0:T(8,128)(2,1)} fusion(bf16[1024,2048]{1,0:T(8,128)(2,1)} %all-gather.11.cloned.1.call-done, bf16[24,8,8,128]{3,2,1,0:T(8,128)(2,1)S(1)} %bitcast.57), kind=kOutput, calls=%fused_computation.1 | convolution fusion | flops 805699584 | bytes 5373952 | tf_op jit(solution)/shard_map/dot_general | solution.py:165
  (10 shorter events, 0.0 us)
Async XLA Ops:
  6.5 175.7 %copy-start = (f32[1024]{0:T(1024)S(1)}, f32[1024]{0:T(1024)}, u32[]{:S(2)}) copy-start(f32[1024]{0:T(1024)} %param.14) | copy-start | bytes 12292
  6.5 23.9 %copy-start.3 = (bf16[128,512]{1,0:T(8,128)(2,1)S(1)}, bf16[128,512]{1,0:T(8,128)(2,1)}, u32[]{:S(2)}) copy-start(bf16[128,512]{1,0:T(8,128)(2,1)} %param.15) | copy-start | bytes 393220
  6.5 31.7 %copy-start.1 = (bf16[1,192,2048]{2,1,0:T(8,128)(2,1)S(1)}, bf16[1,192,2048]{2,1,0:T(8,128)(2,1)}, u32[]{:S(2)}) copy-start(bf16[1,192,2048]{2,1,0:T(8,128)(2,1)} %param.8) | copy-start | bytes 2359300
  6.5 49.4 %all-gather.7.cloned.1.call-start = ((), (), s32[]{:S(2)}) async-start(), calls=%async_computation.5 | async-start | bytes 1179648 | tf_op jit(solution)/shard_map/all_gather | solution.py:115
  15.1 82.0 %all-gather.9.cloned.1.call-start = ((), (), s32[]{:S(2)}) async-start(), calls=%async_computation.6 | async-start | bytes 1179648 | tf_op jit(solution)/shard_map/all_gather | solution.py:116
  21.2 34.7 %copy-start.4 = (f32[2048]{0:T(1024)S(1)}, f32[2048]{0:T(1024)}, u32[]{:S(2)}) copy-start(f32[2048]{0:T(1024)} %param.9) | copy-start | bytes 24580
  21.3 151.2 %all-gather.5.cloned.1.call-start = ((), (), s32[]{:S(2)}) async-start(), calls=%async_computation.4 | async-start | bytes 4718592 | tf_op jit(solution)/shard_map/all_gather | solution.py:122
  30.4 230.6 %all-gather.11.cloned.1.call-start = ((), (), s32[]{:S(2)}) async-start(), calls=%async_computation.7 | async-start | bytes 4718592 | tf_op jit(solution)/shard_map/all_gather | solution.py:167
  58.4 41.1 %all-to-all-start.1 = ((bf16[192,8,32]{0,2,1:T(8,128)(2,1)}), bf16[192,8,32]{0,2,1:T(8,128)(2,1)S(1)}, u32[]{:S(2)}, u32[]{:S(2)}) async-start(bf16[192,8,32]{0,2,1:T(8,128)(2,1)} %bitcast.5), calls=%async_computation.1 | async-start | bytes 262144 | tf_op jit(solution)/shard_map/all_to_all | solution.py:133
  99.6 77.0 %all-to-all-start.2 = ((bf16[192,8,32]{0,2,1:T(8,128)(2,1)}), bf16[192,8,32]{0,2,1:T(8,128)(2,1)S(1)}, u32[]{:S(2)}, u32[]{:S(2)}) async-start(bf16[192,8,32]{0,2,1:T(8,128)(2,1)} %bitcast.12), calls=%async_computation.2 | async-start | bytes 262144 | tf_op jit(solution)/shard_map/all_to_all | solution.py:134
  176.6 33.7 %all-to-all-start = ((bf16[192,8,128]{2,0,1:T(8,128)(2,1)}), bf16[192,8,128]{2,0,1:T(8,128)(2,1)S(1)}, u32[]{:S(2)}, u32[]{:S(2)}) async-start(bf16[192,8,128]{2,0,1:T(8,128)(2,1)} %bitcast.51), calls=%async_computation | async-start | bytes 786432 | tf_op jit(solution)/shard_map/all_to_all | solution.py:132
  180.3 21.3 %collective-permute-start = (bf16[1536,1,32]{2,0,1:T(8,128)(2,1)S(1)}, bf16[1536,1,32]{2,0,1:T(8,128)(2,1)S(1)}, u32[]{:S(2)}, u32[]{:S(2)}) collective-permute-start(bf16[1536,1,32]{2,0,1:T(8,128)(2,1)S(1)} %bitcast.53), channel_id=1, source_target_pairs={{0,4},{4,0},{8,12},{12,8},{16,20},{20,16},{24,28},{28,24},{1,5},{5... | collective-permute-start | bytes 294920 | tf_op jit(solution)/shard_map/ppermute | solution.py:17
  183.1 26.0 %collective-permute-start.1 = (bf16[1536,1,32]{2,0,1:T(8,128)(2,1)S(1)}, bf16[1536,1,32]{2,0,1:T(8,128)(2,1)S(1)}, u32[]{:S(2)}, u32[]{:S(2)}) collective-permute-start(bf16[1536,1,32]{2,0,1:T(8,128)(2,1)S(1)} %bitcast.55), channel_id=1, source_target_pairs={{0,4},{4,0},{8,12},{12,8},{16,20},{20,16},{24,28},{28,24},{1,5},{5... | collective-permute-start | bytes 294920 | tf_op jit(solution)/shard_map/ppermute | solution.py:17
  210.2 0.7 copy-start.2
Sparse Core Ops, SparseCore 0:
  15.2 40.6 all-gather.6
  58.0 38.9 all-gather.8
  99.1 73.3 all-gather.4
  174.5 84.5 all-gather.10

commit v2 on v1

v2 whole, which is shorter than its diff:
```python
import functools

import jax
import jax.numpy as jnp
from jax import lax
from jax.experimental import pallas as pl
from jax.experimental.pallas import tpu as pltpu
from jax.sharding import PartitionSpec as P

HEAD_DIM = 64
MESH = pl.DeviceIdType.MESH
VMEM_SPEC = pl.BlockSpec(memory_space=pltpu.VMEM)


norm_eps = 1e-06


def attention_kernel(block, q_ref, k_ref, v_ref, bias_ref, gain_ref, out_ref):
    heads = bias_ref.shape[0]
    index = pl.program_id(0)
    row = lax.broadcasted_iota(jnp.int32, (block, block), 0)
    column = lax.broadcasted_iota(jnp.int32, (block, block), 1)
    later = jnp.where(row > column, 1.0, 0.0).astype(jnp.bfloat16)
    strict = column < row
    q_heads = [
        q_ref[:, h * HEAD_DIM : (h + 1) * HEAD_DIM] * jnp.bfloat16(HEAD_DIM**-0.5)
        for h in range(heads)
    ]

    def tile(j, h, rest, total, diagonal):
        window = pl.ds(pl.multiple_of(j * block, block), block)
        x = lax.dot_general(
            q_heads[h], k_ref[window, :], (((1,), (1,)), ((), ())),
            preferred_element_type=jnp.float32,
        ) + bias_ref[h : h + 1, window]
        soft = jnp.log(1.0 + jnp.exp(-jnp.abs(x)))
        take = jnp.minimum(x, 0.0) - soft
        keep = jnp.minimum(-x, 0.0) - soft
        if diagonal:
            keep = jnp.where(strict, keep, 0.0)
        high = keep.astype(jnp.bfloat16)
        low = (keep - high.astype(jnp.float32)).astype(jnp.bfloat16)
        after = jnp.dot(high, later, preferred_element_type=jnp.float32) + jnp.dot(
            low, later, preferred_element_type=jnp.float32
        )
        sticks = jnp.exp(take + (after + rest))
        if diagonal:
            sticks = jnp.where(strict, sticks, 0.0)
        total = total + jnp.dot(
            sticks.astype(jnp.bfloat16), v_ref[window, :], preferred_element_type=jnp.float32
        )
        return rest + (after[:, :1] + keep[:, :1]), total

    state = []
    for h in range(heads):
        state += tile(
            index, h, jnp.zeros((block, 1), jnp.float32),
            jnp.zeros((block, HEAD_DIM), jnp.float32), True,
        )

    def step(n, state):
        out = []
        for h in range(heads):
            out += tile(index - 1 - n, h, state[2 * h], state[2 * h + 1], False)
        return tuple(out)

    state = lax.fori_loop(0, index, step, tuple(state))
    for h in range(heads):
        total = state[2 * h + 1]
        lanes = slice(h * HEAD_DIM, (h + 1) * HEAD_DIM)
        scaled = total * lax.rsqrt(jnp.mean(total * total, axis=-1, keepdims=True) + norm_eps)
        out_ref[:, lanes] = (scaled * gain_ref[:, lanes]).astype(jnp.bfloat16)


def attention(q, k, v, bias, gains):
    length, width = q.shape
    block = min(256, length)
    pairs = length * length // 2 * bias.shape[0]
    return pl.pallas_call(
        functools.partial(attention_kernel, block),
        out_shape=jax.ShapeDtypeStruct((length, width), jnp.bfloat16),
        grid=(length // block,),
        in_specs=[
            pl.BlockSpec((block, width), lambda i: (i, 0)),
            pl.BlockSpec(k.shape, lambda i: (0, 0)),
            pl.BlockSpec(v.shape, lambda i: (0, 0)),
            pl.BlockSpec(bias.shape, lambda i: (0, 0)),
            pl.BlockSpec(gains.shape, lambda i: (0, 0)),
        ],
        out_specs=pl.BlockSpec((block, width), lambda i: (i, 0)),
        cost_estimate=pl.CostEstimate(
            flops=pairs * 1500, bytes_accessed=length * width * 8, transcendentals=pairs * 3
        ),
        name="attention",
    )(q, k, v, bias, gains)


def greet(peers):
    barrier = pltpu.get_barrier_semaphore()
    for peer in peers:
        pl.semaphore_signal(barrier, inc=1, device_id=peer, device_id_type=MESH)
    pl.semaphore_wait(barrier, len(peers))


def remote(source, target, send, recv, peer):
    copy = pltpu.make_async_remote_copy(
        src_ref=source, dst_ref=target, send_sem=send, recv_sem=recv,
        device_id=peer, device_id_type=MESH,
    )
    copy.start()
    return copy


def project_kernel(
    zones, group, x_ref, gain_ref, piece_ref, q_ref, kv_ref,
    weights, x_far, normed, kv_parts,
    own_sem, send_z, recv_z, send_x, recv_x, send_c, recv_c, send_y, recv_y,
):
    cores = 2
    columns = lax.axis_size("dp") // cores
    sp, dp = lax.axis_index("sp"), lax.axis_index("dp")
    zone, place = sp // group, sp % group
    column, core = dp // cores, dp % cores
    rows, width = x_ref.shape
    pieces = columns * cores
    depth = width // pieces
    half = depth // 2
    cq = piece_ref.shape[1]
    ck2 = kv_parts.shape[3]

    def at_zone(k):
        return {"sp": lax.rem(zone + k, zones) * group + place}

    def at_column(j):
        return {"dp": lax.rem(column + j, columns) * cores + core}

    def at_place(g):
        return {"sp": zone * group + lax.rem(place + g, group)}

    partner = {"dp": column * cores + (1 - core)}
    greet(
        [at_zone(k) for k in range(1, zones)]
        + [at_column(j) for j in range(1, columns)]
        + [at_place(g) for g in range(1, group)]
        + [partner]
    )

    def slot(k, j, c):
        return k * pieces + j * cores + c

    sent = []
    zone_copies, column_copies, core_copies = {}, {}, {}
    own = pltpu.make_async_copy(piece_ref, weights.at[0], own_sem)
    own.start()

    def spread_own(k):
        source = piece_ref if k == 0 else weights.at[slot(k, 0, 0)]
        for j in range(1, columns):
            column_copies[k, j] = remote(
                source, weights.at[slot(k, j, 0)], send_x.at[k, j], recv_x.at[k, j], at_column(j)
            )
        core_copies[k, 0] = remote(
            source, weights.at[slot(k, 0, 1)], send_c.at[k, 0], recv_c.at[k, 0], partner
        )

    def spread_column(k):
        for j in range(1, columns):
            column_copies[k, j].wait_recv()
            core_copies[k, j] = remote(
                weights.at[slot(k, j, 0)], weights.at[slot(k, j, 1)],
                send_c.at[k, j], recv_c.at[k, j], partner,
            )

    for k in range(1, zones):
        zone_copies[k] = remote(
            piece_ref, weights.at[slot(k, 0, 0)], send_z.at[k], recv_z.at[k], at_zone(k)
        )
    spread_own(0)
    place_copies = [
        remote(x_ref, x_far.at[g], send_y.at[g], recv_y.at[g], at_place(g))
        for g in range(1, group)
    ]

    step = 16

    def normalize(source, g):
        def chunk(n, carry):
            here = pl.ds(pl.multiple_of(n * step, step), step)
            wide = source[here, :].astype(jnp.float32)
            scale = lax.rsqrt(jnp.mean(wide * wide, axis=-1, keepdims=True) + norm_eps)
            for d in range(pieces):
                j, c = d // cores, d % cores
                index = lax.rem(column - j + columns, columns) * cores + (
                    core if c == 0 else 1 - core
                )
                for s in range(2):
                    lanes = pl.ds(pl.multiple_of(index * depth + s * half, half), half)
                    part = source[here, lanes].astype(jnp.float32) * scale * gain_ref[:, lanes]
                    normed[g, s, here, d * half : (d + 1) * half] = part.astype(jnp.bfloat16)
            return carry

        lax.fori_loop(0, rows // step, chunk, 0)

    def project(k, g):
        zone_of = lax.rem(zone - k + zones, zones)
        place_of = lax.rem(place - g + group, group)
        first = k * pieces
        key_weights = weights[pl.ds(first, pieces), depth : depth + half, :]
        key_weights = key_weights.reshape(pieces * half, cq)
        both = []
        for s in range(2):
            query_weights = weights[pl.ds(first, pieces), s * half : (s + 1) * half, :]
            query_weights = query_weights.reshape(pieces * half, cq)
            both.append(
                jnp.dot(
                    normed[g, s], jnp.concatenate([query_weights, key_weights], axis=1),
                    preferred_element_type=jnp.float32,
                )
            )
        q_ref[zone_of, place_of] = (both[0][:, :cq] + both[1][:, :cq]).astype(jnp.bfloat16)
        kv_parts[zone_of, place_of] = (
            both[0][:, cq : cq + ck2] + both[1][:, cq + ck2 : cq + 2 * ck2]
        )

    def settle(k):
        for j in range(columns):
            core_copies[k, j].wait_recv()
        project(k, 0)

    normalize(x_ref, 0)
    own.wait()
    for k in range(zones):
        if k > 0:
            zone_copies[k].wait_recv()
            spread_own(k)
            spread_column(k - 1)
        if k > 1:
            settle(k - 2)
    spread_column(zones - 1)
    for k in range(max(zones - 2, 0), zones):
        settle(k)
    for g in range(1, group):
        place_copies[g - 1].wait_recv()
        normalize(x_far.at[g], g)

        def later(k, carry):
            project(k, g)
            return carry

        lax.fori_loop(0, zones, later, 0)
    for z in range(zones):
        kv_ref[z] = jnp.concatenate(
            [kv_parts[z, g] for g in range(group)], axis=1
        ).astype(jnp.bfloat16)
    for copies in (zone_copies, column_copies, core_copies):
        for copy in copies.values():
            copy.wait_send()
    for copy in place_copies:
        copy.wait_send()


def project(x, gain, piece, zones, group, ck2):
    rows, width = x.shape
    pieces = lax.axis_size("dp")
    columns = pieces // 2
    cq = piece.shape[1]
    dma = pltpu.SemaphoreType.DMA
    return pl.pallas_call(
        functools.partial(project_kernel, zones, group),
        out_shape=(
            jax.ShapeDtypeStruct((zones, group, rows, cq), jnp.bfloat16),
            jax.ShapeDtypeStruct((zones, rows, group * ck2), jnp.bfloat16),
        ),
        in_specs=[VMEM_SPEC] * 3,
        out_specs=[VMEM_SPEC] * 2,
        scratch_shapes=[
            pltpu.VMEM((zones * pieces,) + piece.shape, jnp.bfloat16),
            pltpu.VMEM((group, rows, width), jnp.bfloat16),
            pltpu.VMEM((group, 2, rows, width // 2), jnp.bfloat16),
            pltpu.VMEM((zones, group, rows, ck2), jnp.float32),
            dma,
            dma((zones,)), dma((zones,)),
            dma((zones, columns)), dma((zones, columns)),
            dma((zones, columns)), dma((zones, columns)),
            dma((group,)), dma((group,)),
        ],
        compiler_params=pltpu.CompilerParams(collective_id=0, has_side_effects=True),
        name="project",
    )(x, gain, piece)


def exchange_kernel(
    zones, group, q_ref, kv_ref, q_out, kv_out, own_sem, send_q, recv_q, send_k, recv_k
):
    sp = lax.axis_index("sp")
    zone, place = sp // group, sp % group

    def at(k, g):
        return {"sp": lax.rem(zone + k, zones) * group + lax.rem(place + g, group)}

    others = [(k, g) for k in range(zones) for g in range(group) if k + g > 0]
    greet([at(k, g) for k, g in others])
    local = [
        pltpu.make_async_copy(q_ref.at[zone], q_out.at[zone], own_sem.at[0]),
        pltpu.make_async_copy(kv_ref.at[zone], kv_out.at[zone, place], own_sem.at[1]),
    ]
    for copy in local:
        copy.start()
    copies = []
    for k, g in others:
        there = lax.rem(zone + k, zones)
        if g == 0:
            copies.append(
                remote(q_ref.at[there], q_out.at[zone], send_q.at[k], recv_q.at[k], at(k, g))
            )
        copies.append(
            remote(
                kv_ref.at[there], kv_out.at[zone, place],
                send_k.at[k, g], recv_k.at[k, g], at(k, g),
            )
        )
    for copy in local + copies:
        copy.wait()


def exchange(q, kv, zones, group):
    dma = pltpu.SemaphoreType.DMA
    return pl.pallas_call(
        functools.partial(exchange_kernel, zones, group),
        out_shape=(
            jax.ShapeDtypeStruct(q.shape, q.dtype),
            jax.ShapeDtypeStruct((zones, group) + kv.shape[1:], kv.dtype),
        ),
        in_specs=[VMEM_SPEC] * 2,
        out_specs=[VMEM_SPEC] * 2,
        scratch_shapes=[
            dma((2,)), dma((zones,)), dma((zones,)), dma((zones, group)), dma((zones, group)),
        ],
        compiler_params=pltpu.CompilerParams(collective_id=1, has_side_effects=True),
        name="exchange",
    )(q, kv)


def finish_kernel(head_ref, w_ref, out_ref, arrived, joined, own_sem, send, recv):
    size = lax.axis_size("sp")
    sp = lax.axis_index("sp")
    rows, width = out_ref.shape
    cq = head_ref.shape[2]

    def at(k):
        return {"sp": lax.rem(sp + k, size)}

    greet([at(k) for k in range(1, size)])
    own = pltpu.make_async_copy(head_ref.at[sp], arrived.at[sp], own_sem)
    own.start()
    copies = [
        remote(
            head_ref.at[lax.rem(sp + k, size)], arrived.at[sp], send.at[k], recv.at[k], at(k)
        )
        for k in range(1, size)
    ]
    for copy in [own] + copies:
        copy.wait()
    for k in range(size):
        joined[:, k * cq : (k + 1) * cq] = arrived[k]
    tile = min(512, width)

    def step(n, carry):
        lanes = pl.ds(pl.multiple_of(n * tile, tile), tile)
        out_ref[:, lanes] = jnp.dot(
            joined[...], w_ref[:, lanes], preferred_element_type=jnp.float32
        ).astype(jnp.bfloat16)
        return carry

    lax.fori_loop(0, width // tile, step, 0)


def finish(heads, w_out):
    size, rows, cq = heads.shape
    dma = pltpu.SemaphoreType.DMA
    return pl.pallas_call(
        finish_kernel,
        out_shape=jax.ShapeDtypeStruct((rows, w_out.shape[1]), jnp.bfloat16),
        in_specs=[VMEM_SPEC] * 2,
        out_specs=VMEM_SPEC,
        scratch_shapes=[
            pltpu.VMEM(heads.shape, jnp.bfloat16),
            pltpu.VMEM((rows, size * cq), jnp.bfloat16),
            dma, dma((size,)), dma((size,)),
        ],
        compiler_params=pltpu.CompilerParams(collective_id=2, has_side_effects=True),
        name="finish",
    )(heads, w_out)


def body(inputs, in_gain, w_query, w_key, w_value, key_bias, out_gain, w_out):
    width_sp = lax.axis_size("sp")
    own_index = lax.axis_index("sp")
    rows = inputs.shape[1]
    heads_here = key_bias.shape[2]
    cq = w_query.shape[1]
    ck = w_key.shape[1]
    group = HEAD_DIM // ck
    zones = width_sp // group
    depth = w_query.shape[0]
    pair = jnp.concatenate([w_key, w_value], axis=1)
    piece = jnp.concatenate(
        [w_query, jnp.concatenate([pair[: depth // 2], pair[depth // 2 :]], axis=1)], axis=0
    )
    w_full = lax.all_gather(
        lax.all_gather(w_out, "dp", axis=1, tiled=True), "sp", axis=0, tiled=True
    )
    q_parts, kv_parts = project(inputs[0], in_gain[None], piece, zones, group, 2 * ck)
    q_all, kv_all = exchange(q_parts, kv_parts, zones, group)
    length = width_sp * rows
    kv = kv_all.reshape(zones, group, rows, group, 2, ck).transpose(4, 0, 3, 2, 1, 5)
    kv = kv.reshape(2, length, HEAD_DIM)
    gains = lax.dynamic_slice_in_dim(out_gain, own_index * cq, cq, 0).reshape(1, cq)
    head_out = attention(q_all.reshape(length, cq), kv[0], kv[1], key_bias[0].T, gains)
    return finish(head_out.reshape(width_sp, rows, cq), w_full)[None]


def solution(mesh):
    placed = (
        P("dp", "sp", None),
        P(),
        P("dp", "sp"),
        P("dp", "sp"),
        P("dp", "sp"),
        P("dp", None, "sp"),
        P(),
        P("sp", "dp"),
    )
    return jax.shard_map(
        body, mesh=mesh, in_specs=placed, out_specs=P("dp", "sp", None), check_vma=False
    )
```

time: 272 us -> 173 us (0.64)
  waiting for transfers between devices: 147 us -> 0.02 us
  Pallas kernels: 26.5 us -> 139 us
  blocking collectives: 51.7 us -> 10.4 us
  starting transfers between devices: 12.5 us -> 0.01 us
  matrix products: 10.8 us -> 0 us
  local copies, waits for them, and re-layouts: 5.42 us -> 8.52 us
  other arithmetic: 4.55 us -> 1.79 us
    all_gather x4 -> x1, waiting for transfers between devices: 122 us -> 0.01 us  [body(): lax.all_gather(lax.all_gather(w_out, 'dp', axis=1, tiled=True), 'sp', axi...]
    pallas_call x0 -> x3, Pallas kernels: none -> 112 us  [the longest x1 44.1 us: exchange(): pl.pallas_call(functools.partial(exchange_kernel, zones, group), out_shap...]
    ppermute x2 -> x0, waiting for transfers between devices: 24.6 us -> none  [from_partner(): lax.ppermute(value, axis, [(i, i ^ 1 << distance) for i in range(lax.axis...]
    all_gather x3 -> x0, blocking collectives: 23.7 us -> none  [the longest x1 9.1 us: body(): lax.all_gather(w_query, 'dp', axis=0, tiled=True)]
    all_to_all x1 -> x0, blocking collectives: 20.3 us -> none  [body(): lax.all_to_all(head_out, 'sp', split_axis=0, concat_axis=1, tiled=True)]
    dot_general x4 -> x0, matrix products: 10.8 us -> none  [the longest x1 4.06 us: body(): jnp.dot(returned, lax.all_gather(w_out, 'sp', axis=0, tiled=True), prefer...]
    all_to_all x3 -> x0, starting transfers between devices: 10.2 us -> none  [the longest x1 3.45 us: body(): lax.all_to_all(query_slots, 'sp', split_axis=1, concat_axis=0, tiled=True)]
  transfers between devices with their start and end apart: 9 -> 1, of which waited for: 5 -> 0; matrix products, arithmetic and copies ran while one was open for 6% -> 5% of each run, Pallas kernels for 10% -> 64%
where the time goes in v2:
time: 173 us
  Pallas kernels  139 us (80%)
  between operations  13.5 us (8%)
  blocking collectives  10.4 us (6%)
  local copies, waits for them, and re-layouts  8.52 us (5%)
  other arithmetic  1.79 us (1%)
    pallas_call x1, Pallas kernels, exchange(): pl.pallas_call(functools.partial(exchange_kernel, zones, group), out_shap...  44.1 us
    pallas_call x1, Pallas kernels, project(): pl.pallas_call(functools.partial(project_kernel, zones, group), out_shape...  40 us
    pallas_call x1, Pallas kernels, finish(): pl.pallas_call(finish_kernel, out_shape=jax.ShapeDtypeStruct((rows, w_out...  28.2 us
    pallas_call x1, Pallas kernels, attention(): pl.pallas_call(functools.partial(attention_kernel, block), out_shape=jax....  26.5 us
    all_gather x1, blocking collectives, body(): lax.all_gather(w_out, 'dp', axis=1, tiled=True)  10.4 us
    unnamed x5, local copies, waits for them, and re-layouts  3.86 us
  transfers between devices with their start and end apart: 1, of which 0 were waited for; matrix products, arithmetic and copies ran while one was open for 5% of the time, Pallas kernels for 64%

profile of v2, /device:TPU:0, one launch (start us, length us, event | category | flops | bytes accessed | tf_op | source)
XLA Modules:
  0.0 172.9 jit_solution(2710817525142984759)
XLA Ops:
  6.5 0.0 copy-start
  6.5 0.0 all-gather.2.cloned.1.call-start
  6.5 10.4 %all_gather.6 = bf16[128,2048]{1,0:T(8,128)(2,1)} all-gather(bf16[128,512]{1,0:T(8,128)(2,1)} %param.15), channel_id=1, replica_groups=mesh['sp'=8,'dp'=4] {'dp'}, dimensions={1}, use_global_device_ids=true | all-gather | bytes 655360 | tf_op jit(solution)/shard_map/all_gather | solution.py:411
  16.9 0.0 all-gather.2.cloned.1.call-update
  16.9 0.9 copy.12
  17.8 0.9 copy.13
  18.7 0.1 fusion.8
  18.8 1.7 fusion.7.piece_ref
  20.5 40.0 %project.1 = (bf16[4,2,192,128]{3,2,1,0:T(8,128)(2,1)}, bf16[4,192,128]{2,1,0:T(8,128)(2,1)}) custom-call(bf16[192,2048]{1,0:T(8,128)(2,1)} %bitcast.19, f32[1,2048]{1,0:T(1,128)} %bitcast.21, bf16[768,128]{1,0:T(8,128)(2,1)} %fusion.7.piece_ref), custom_call_target="tpu_custom_call" | custom-call | tf_op jit(solution)/shard_map/project/pallas_call | solution.py:268
  60.5 44.1 %exchange.1 = (bf16[4,2,192,128]{3,2,1,0:T(8,128)(2,1)}, bf16[4,2,192,128]{3,2,1,0:T(8,128)(2,1)}) custom-call(bf16[4,2,192,128]{3,2,1,0:T(8,128)(2,1)} %get-tuple-element.9.q_ref, bf16[4,192,128]{2,1,0:T(8,128)(2,1)} %get-tuple-element.10.kv_ref), custom_call_target="tpu_custom_call" | custom-call | tf_op jit(solution)/shard_map/exchange/pallas_call | solution.py:328
  104.6 1.2 copy.14
  105.9 0.3 copy.16
  106.1 0.2 squeeze.14
  106.4 0.9 copy.18.v_ref
  107.3 0.3 copy.15
  107.6 0.2 squeeze.13
  107.8 0.9 copy.17.k_ref
  108.7 0.0 copy-done
  108.7 0.6 dynamic-slice_bitcast_fusion.gain_ref
  109.3 26.5 %attention.1 = bf16[1536,128]{1,0:T(8,128)(2,1)} custom-call(bf16[1536,128]{1,0:T(8,128)(2,1)} %bitcast.22, bf16[1536,64]{1,0:T(8,128)(2,1)} %copy.17.k_ref, bf16[1536,64]{1,0:T(8,128)(2,1)} %copy.18.v_ref, f32[2,1536]{1,0:T(2,128)} %bitcast.23, f32[1,128]{1,0:T(1,128)} %dynamic-slice_bitcast_fusion.gain_ref), custom_call_target="tpu_custom_call" | custom-call | flops 3538944000 | bytes 1572864 | tf_op jit(solution)/shard_map/attention/pallas_call | solution.py:79
  135.8 0.0 all-gather.2.cloned.1.call-done.w_ref
  135.8 28.2 %finish.1 = bf16[192,2048]{1,0:T(8,128)(2,1)} custom-call(bf16[8,192,128]{2,1,0:T(8,128)(2,1)} %bitcast.20, bf16[1024,2048]{1,0:T(8,128)(2,1)} %all-gather.2.cloned.1.call-done.w_ref), custom_call_target="tpu_custom_call" | custom-call | tf_op jit(solution)/shard_map/finish/pallas_call | solution.py:381
  164.0 2.1 %copy.20 = bf16[1,192,2048]{2,1,0:T(8,128)(2,1)} copy(bf16[1,192,2048]{2,1,0:T(8,128)(2,1)} %bitcast.17) | data formatting | bytes 1572864
  (1 shorter events, 0.0 us)
Async XLA Ops:
  6.5 102.2 %copy-start = (f32[1024]{0:T(1024)S(1)}, f32[1024]{0:T(1024)}, u32[]{:S(2)}) copy-start(f32[1024]{0:T(1024)} %param.14) | copy-start | bytes 12292
  6.5 129.3 %all-gather.2.cloned.1.call-start = ((), (), s32[]{:S(2)}) async-start(), calls=%async_computation | async-start | bytes 4718592 | tf_op jit(solution)/shard_map/all_gather | solution.py:410
Sparse Core Ops, SparseCore 0:
  17.1 102.3 all-gather.1

commit v3 on v2

v3 whole, which is shorter than its diff:
```python
import functools

import jax
import jax.numpy as jnp
from jax import lax
from jax.experimental import pallas as pl
from jax.experimental.pallas import tpu as pltpu
from jax.sharding import PartitionSpec as P

HEAD_DIM = 64
MESH = pl.DeviceIdType.MESH
VMEM_SPEC = pl.BlockSpec(memory_space=pltpu.VMEM)


norm_eps = 1e-06


def greet(peers):
    barrier = pltpu.get_barrier_semaphore()
    for peer in peers:
        pl.semaphore_signal(barrier, inc=1, device_id=peer, device_id_type=MESH)
    pl.semaphore_wait(barrier, len(peers))


def remote(source, target, send, recv, peer):
    copy = pltpu.make_async_remote_copy(
        src_ref=source, dst_ref=target, send_sem=send, recv_sem=recv,
        device_id=peer, device_id_type=MESH,
    )
    copy.start()
    return copy


def project_kernel(
    zones, group, x_ref, gain_ref, piece_ref, q_ref, kv_ref,
    weights, x_far, normed, kv_parts,
    own_sem, send_z, recv_z, send_x, recv_x, send_c, recv_c, send_y, recv_y,
):
    cores = 2
    columns = lax.axis_size("dp") // cores
    sp, dp = lax.axis_index("sp"), lax.axis_index("dp")
    zone, place = sp // group, sp % group
    column, core = dp // cores, dp % cores
    rows, width = x_ref.shape
    pieces = columns * cores
    depth = width // pieces
    half = depth // 2
    cq = piece_ref.shape[1]
    ck2 = kv_parts.shape[3]

    def at_zone(k):
        return {"sp": lax.rem(zone + k, zones) * group + place}

    def at_column(j):
        return {"dp": lax.rem(column + j, columns) * cores + core}

    def at_place(g):
        return {"sp": zone * group + lax.rem(place + g, group)}

    partner = {"dp": column * cores + (1 - core)}
    greet(
        [at_zone(k) for k in range(1, zones)]
        + [at_column(j) for j in range(1, columns)]
        + [at_place(g) for g in range(1, group)]
        + [partner]
    )

    def slot(k, j, c):
        return k * pieces + j * cores + c

    sent = []
    zone_copies, column_copies, core_copies = {}, {}, {}
    own = pltpu.make_async_copy(piece_ref, weights.at[0], own_sem)
    own.start()

    def spread_own(k):
        source = piece_ref if k == 0 else weights.at[slot(k, 0, 0)]
        for j in range(1, columns):
            column_copies[k, j] = remote(
                source, weights.at[slot(k, j, 0)], send_x.at[k, j], recv_x.at[k, j], at_column(j)
            )
        core_copies[k, 0] = remote(
            source, weights.at[slot(k, 0, 1)], send_c.at[k, 0], recv_c.at[k, 0], partner
        )

    def spread_column(k):
        for j in range(1, columns):
            column_copies[k, j].wait_recv()
            core_copies[k, j] = remote(
                weights.at[slot(k, j, 0)], weights.at[slot(k, j, 1)],
                send_c.at[k, j], recv_c.at[k, j], partner,
            )

    for k in range(1, zones):
        zone_copies[k] = remote(
            piece_ref, weights.at[slot(k, 0, 0)], send_z.at[k], recv_z.at[k], at_zone(k)
        )
    spread_own(0)
    place_copies = [
        remote(x_ref, x_far.at[g], send_y.at[g], recv_y.at[g], at_place(g))
        for g in range(1, group)
    ]

    step = 16

    def normalize(source, g):
        def chunk(n, carry):
            here = pl.ds(pl.multiple_of(n * step, step), step)
            wide = source[here, :].astype(jnp.float32)
            scale = lax.rsqrt(jnp.mean(wide * wide, axis=-1, keepdims=True) + norm_eps)
            for d in range(pieces):
                j, c = d // cores, d % cores
                index = lax.rem(column - j + columns, columns) * cores + (
                    core if c == 0 else 1 - core
                )
                for s in range(2):
                    lanes = pl.ds(pl.multiple_of(index * depth + s * half, half), half)
                    part = source[here, lanes].astype(jnp.float32) * scale * gain_ref[:, lanes]
                    normed[g, s, here, d * half : (d + 1) * half] = part.astype(jnp.bfloat16)
            return carry

        lax.fori_loop(0, rows // step, chunk, 0)

    def project(k, g):
        zone_of = lax.rem(zone - k + zones, zones)
        place_of = lax.rem(place - g + group, group)
        first = k * pieces
        key_weights = weights[pl.ds(first, pieces), depth : depth + half, :]
        key_weights = key_weights.reshape(pieces * half, cq)
        both = []
        for s in range(2):
            query_weights = weights[pl.ds(first, pieces), s * half : (s + 1) * half, :]
            query_weights = query_weights.reshape(pieces * half, cq)
            both.append(
                jnp.dot(
                    normed[g, s], jnp.concatenate([query_weights, key_weights], axis=1),
                    preferred_element_type=jnp.float32,
                )
            )
        target = pl.ds(pl.multiple_of(place_of * rows, rows), rows)
        q_ref[zone_of, target, :] = (both[0][:, :cq] + both[1][:, :cq]).astype(jnp.bfloat16)
        kv_parts[zone_of, place_of] = (
            both[0][:, cq : cq + ck2] + both[1][:, cq + ck2 : cq + 2 * ck2]
        )

    def settle(k):
        for j in range(columns):
            core_copies[k, j].wait_recv()
        project(k, 0)

    normalize(x_ref, 0)
    own.wait()
    for k in range(zones):
        if k > 0:
            zone_copies[k].wait_recv()
            spread_own(k)
            spread_column(k - 1)
        if k > 1:
            settle(k - 2)
    spread_column(zones - 1)
    for k in range(max(zones - 2, 0), zones):
        settle(k)
    for g in range(1, group):
        place_copies[g - 1].wait_recv()
        normalize(x_far.at[g], g)

        def later(k, carry):
            project(k, g)
            return carry

        lax.fori_loop(0, zones, later, 0)
    for z in range(zones):
        kv_ref[z] = jnp.concatenate(
            [kv_parts[z, g] for g in range(group)], axis=1
        ).astype(jnp.bfloat16)
    for copies in (zone_copies, column_copies, core_copies):
        for copy in copies.values():
            copy.wait_send()
    for copy in place_copies:
        copy.wait_send()


def project(x, gain, piece, zones, group, ck2):
    rows, width = x.shape
    pieces = lax.axis_size("dp")
    columns = pieces // 2
    cq = piece.shape[1]
    dma = pltpu.SemaphoreType.DMA
    return pl.pallas_call(
        functools.partial(project_kernel, zones, group),
        out_shape=(
            jax.ShapeDtypeStruct((zones, group * rows, cq), jnp.bfloat16),
            jax.ShapeDtypeStruct((zones, rows, group * ck2), jnp.bfloat16),
        ),
        in_specs=[VMEM_SPEC] * 3,
        out_specs=[VMEM_SPEC] * 2,
        scratch_shapes=[
            pltpu.VMEM((zones * pieces,) + piece.shape, jnp.bfloat16),
            pltpu.VMEM((group, rows, width), jnp.bfloat16),
            pltpu.VMEM((group, 2, rows, width // 2), jnp.bfloat16),
            pltpu.VMEM((zones, group, rows, ck2), jnp.float32),
            dma,
            dma((zones,)), dma((zones,)),
            dma((zones, columns)), dma((zones, columns)),
            dma((zones, columns)), dma((zones, columns)),
            dma((group,)), dma((group,)),
        ],
        compiler_params=pltpu.CompilerParams(collective_id=0, has_side_effects=True),
        name="project",
    )(x, gain, piece)


def mixer_kernel(
    zones, group, block, q_ref, kv_ref, w_ref, bias_ref, gain_ref, out_ref,
    q_all, kv_all, k_all, v_all, w_all, head, arrived, joined,
    own_sem, send_q, recv_q, send_k, recv_k, send_z, recv_z, send_x, recv_x,
    send_y, recv_y, send_c, recv_c, send_h, recv_h,
):
    cores = 2
    size = zones * group
    columns = lax.axis_size("dp") // cores
    sp, dp = lax.axis_index("sp"), lax.axis_index("dp")
    zone, place = sp // group, sp % group
    column, core = dp // cores, dp % cores
    rows, width = out_ref.shape
    length, cq = q_all.shape
    heads = bias_ref.shape[0]
    span = group * rows
    ck = HEAD_DIM // group
    w_cols = w_ref.shape[1]

    def at(k, g):
        return {"sp": lax.rem(zone + k, zones) * group + lax.rem(place + g, group)}

    def at_column(j):
        return {"dp": lax.rem(column + j, columns) * cores + core}

    partner = {"dp": column * cores + (1 - core)}
    others = [(k, g) for k in range(zones) for g in range(group) if k + g > 0]
    greet([at(k, g) for k, g in others] + [at_column(j) for j in range(1, columns)] + [partner])

    here = pl.ds(pl.multiple_of(zone * span, span), span)
    local = [
        pltpu.make_async_copy(q_ref.at[zone], q_all.at[here, :], own_sem.at[0]),
        pltpu.make_async_copy(kv_ref.at[zone], kv_all.at[zone, place], own_sem.at[1]),
    ]
    own_lanes = pl.ds(pl.multiple_of(dp * w_cols, w_cols), w_cols)
    own_weight = pltpu.make_async_copy(w_ref, w_all.at[sp, :, own_lanes], own_sem.at[2])
    for copy in local + [own_weight]:
        copy.start()
    copies = []
    for k, g in others:
        there = lax.rem(zone + k, zones)
        if g == 0:
            copies.append(
                remote(q_ref.at[there], q_all.at[here, :], send_q.at[k], recv_q.at[k], at(k, g))
            )
        copies.append(
            remote(
                kv_ref.at[there], kv_all.at[zone, place],
                send_k.at[k, g], recv_k.at[k, g], at(k, g),
            )
        )

    def weight(k, j, g):
        row = lax.rem(zone - k + zones, zones) * group + lax.rem(place - g + group, group)
        lane = lax.rem(column - j + columns, columns) * cores + core
        return w_all.at[row, :, pl.ds(pl.multiple_of(lane * w_cols, w_cols), w_cols)]

    flights = {}

    def to_core(k, j, g):
        source = w_ref if k + j + g == 0 else weight(k, j, g)
        flights["c", k, j, g] = remote(
            source, weight(k, j, g), send_c.at[k, j, g], recv_c.at[k, j, g], partner
        )

    def to_places(k, j):
        source = w_ref if k + j == 0 else weight(k, j, 0)
        for g in range(1, group):
            flights["y", k, j, g] = remote(
                source, weight(k, j, 0), send_y.at[k, j, g], recv_y.at[k, j, g], at(0, g)
            )
        to_core(k, j, 0)

    def to_columns(k):
        source = w_ref if k == 0 else weight(k, 0, 0)
        for j in range(1, columns):
            flights["x", k, j] = remote(
                source, weight(k, 0, 0), send_x.at[k, j], recv_x.at[k, j], at_column(j)
            )
        to_places(k, 0)

    def zone_event(k):
        flights["z", k].wait_recv()
        to_columns(k)

    def column_event(k):
        for j in range(1, columns):
            flights["x", k, j].wait_recv()
            to_places(k, j)

    def place_event(k):
        for j in range(columns):
            for g in range(1, group):
                flights["y", k, j, g].wait_recv()
                to_core(k, j, g)

    for k in range(1, zones):
        flights["z", k] = remote(w_ref, weight(0, 0, 0), send_z.at[k], recv_z.at[k], at(k, 0))
    to_columns(0)

    for copy in local + copies:
        copy.wait()
    for z in range(zones):
        for g in range(group):
            target = slice((z * group + g) * rows, (z * group + g + 1) * rows)
            first = g * 2 * ck
            parts = [kv_all[z, y] for y in range(group)]
            k_all[target, :] = jnp.concatenate([p[:, first : first + ck] for p in parts], axis=1)
            v_all[target, :] = jnp.concatenate(
                [p[:, first + ck : first + 2 * ck] for p in parts], axis=1
            )

    row = lax.broadcasted_iota(jnp.int32, (block, block), 0)
    lane = lax.broadcasted_iota(jnp.int32, (block, block), 1)
    later = jnp.where(row > lane, 1.0, 0.0).astype(jnp.bfloat16)
    strict = lane < row

    def tile(i, j, h, rest, total, diagonal):
        window = pl.ds(pl.multiple_of(j * block, block), block)
        lanes = slice(h * HEAD_DIM, (h + 1) * HEAD_DIM)
        q = q_all[i * block : (i + 1) * block, lanes] * jnp.bfloat16(HEAD_DIM**-0.5)
        x = lax.dot_general(
            q, k_all[window, :], (((1,), (1,)), ((), ())), preferred_element_type=jnp.float32
        ) + bias_ref[h : h + 1, window]
        soft = jnp.log(1.0 + jnp.exp(-jnp.abs(x)))
        take = jnp.minimum(x, 0.0) - soft
        keep = jnp.minimum(-x, 0.0) - soft
        if diagonal:
            keep = jnp.where(strict, keep, 0.0)
        high = keep.astype(jnp.bfloat16)
        low = (keep - high.astype(jnp.float32)).astype(jnp.bfloat16)
        after = jnp.dot(high, later, preferred_element_type=jnp.float32) + jnp.dot(
            low, later, preferred_element_type=jnp.float32
        )
        sticks = jnp.exp(take + (after + rest))
        if diagonal:
            sticks = jnp.where(strict, sticks, 0.0)
        total = total + jnp.dot(
            sticks.astype(jnp.bfloat16), v_all[window, :], preferred_element_type=jnp.float32
        )
        return rest + (after[:, :1] + keep[:, :1]), total

    events = []
    for n in range(1, zones + 2):
        now = []
        if n < zones:
            now.append(functools.partial(zone_event, n))
        if n <= zones:
            now.append(functools.partial(column_event, n - 1))
        if 0 <= n - 3 < zones:
            now.append(functools.partial(place_event, n - 3))
        events.append((n if n <= 3 else 2 * n - 3, now))
    events.append((10**9, [functools.partial(place_event, zones - 1)]))
    ready = []
    point = [0]

    def send_head(s):
        return pltpu.make_async_remote_copy(
            src_ref=head.at[s * rows : (s + 1) * rows, :], dst_ref=arrived.at[sp],
            send_sem=send_h.at[s], recv_sem=recv_h.at[sp],
            device_id={"sp": s}, device_id_type=MESH,
        )

    def receive_head(s):
        return pltpu.make_async_remote_copy(
            src_ref=head.at[s * rows : (s + 1) * rows, :], dst_ref=arrived.at[s],
            send_sem=send_h.at[s], recv_sem=recv_h.at[s],
            device_id={"sp": s}, device_id_type=MESH,
        )

    def unless_own(s, act):
        @pl.when(sp != s)
        def _():
            act()

    def relay(final=False):
        while events and (final or events[0][0] <= point[0]):
            for event in events.pop(0)[1]:
                event()
        while ready:
            s = ready.pop(0)
            unless_own(s, lambda s=s: send_head(s).start())
        point[0] += 1

    done = 0
    for i in range(length // block):
        state = []
        for h in range(heads):
            state += tile(
                i, i, h, jnp.zeros((block, 1), jnp.float32),
                jnp.zeros((block, HEAD_DIM), jnp.float32), True,
            )
        state = tuple(state)
        begin = 0
        while begin < i:
            end = min(begin + (2 if begin == 0 else 3), i)

            def step(n, state, i=i):
                out = []
                for h in range(heads):
                    out += tile(i, i - 1 - n, h, state[2 * h], state[2 * h + 1], False)
                return tuple(out)

            state = lax.fori_loop(begin, end, step, state)
            begin = end
            if begin < i:
                relay()
        for h in range(heads):
            total = state[2 * h + 1]
            lanes = slice(h * HEAD_DIM, (h + 1) * HEAD_DIM)
            scaled = total * lax.rsqrt(jnp.mean(total * total, axis=-1, keepdims=True) + norm_eps)
            head[i * block : (i + 1) * block, lanes] = (
                scaled * gain_ref[:, lanes]
            ).astype(jnp.bfloat16)
        if i + 1 < length // block:
            relay()
        while (done + 1) * rows <= (i + 1) * block:
            ready.append(done)
            done += 1
    relay(final=True)
    mine = pltpu.make_async_copy(
        head.at[pl.ds(pl.multiple_of(sp * rows, rows), rows), :], arrived.at[sp], own_sem.at[3]
    )
    mine.start()
    own_weight.wait()
    for key, copy in flights.items():
        if key[0] == "c":
            copy.wait_recv()
    mine.wait()
    for s in range(size):
        unless_own(s, lambda s=s: receive_head(s).wait_recv())
    for s in range(size):
        joined[:, s * cq : (s + 1) * cq] = arrived[s]
    wide = min(512, width)

    def multiply(n, carry):
        lanes = pl.ds(pl.multiple_of(n * wide, wide), wide)
        weights = w_all[:, :, lanes].reshape(size * cq, wide)
        out_ref[:, lanes] = jnp.dot(
            joined[...], weights, preferred_element_type=jnp.float32
        ).astype(jnp.bfloat16)
        return carry

    lax.fori_loop(0, width // wide, multiply, 0)
    for copy in flights.values():
        copy.wait_send()
    for s in range(size):
        unless_own(s, lambda s=s: send_head(s).wait_send())


def mixer(q, kv, w_out, bias, gains, zones, group):
    span, cq = q.shape[1:]
    rows = span // group
    size = zones * group
    length = size * rows
    cores = 2
    columns = lax.axis_size("dp") // cores
    width = w_out.shape[1] * columns * cores
    block = min(256, length)
    dma = pltpu.SemaphoreType.DMA
    grid3 = (zones, columns, group)
    return pl.pallas_call(
        functools.partial(mixer_kernel, zones, group, block),
        out_shape=jax.ShapeDtypeStruct((rows, width), jnp.bfloat16),
        in_specs=[VMEM_SPEC] * 5,
        out_specs=VMEM_SPEC,
        scratch_shapes=[
            pltpu.VMEM((length, cq), jnp.bfloat16),
            pltpu.VMEM((zones, group) + kv.shape[1:], jnp.bfloat16),
            pltpu.VMEM((length, HEAD_DIM), jnp.bfloat16),
            pltpu.VMEM((length, HEAD_DIM), jnp.bfloat16),
            pltpu.VMEM((size, w_out.shape[0], width), jnp.bfloat16),
            pltpu.VMEM((length, cq), jnp.bfloat16),
            pltpu.VMEM((size, rows, cq), jnp.bfloat16),
            pltpu.VMEM((rows, size * cq), jnp.bfloat16),
            dma((4,)),
            dma((zones,)), dma((zones,)),
            dma((zones, group)), dma((zones, group)),
            dma((zones,)), dma((zones,)),
            dma((zones, columns)), dma((zones, columns)),
            dma(grid3), dma(grid3), dma(grid3), dma(grid3),
            dma((size,)), dma((size,)),
        ],
        compiler_params=pltpu.CompilerParams(collective_id=1, has_side_effects=True),
        name="mixer",
    )(q, kv, w_out, bias, gains)


def body(inputs, in_gain, w_query, w_key, w_value, key_bias, out_gain, w_out):
    width_sp = lax.axis_size("sp")
    own_index = lax.axis_index("sp")
    cq = w_query.shape[1]
    ck = w_key.shape[1]
    group = HEAD_DIM // ck
    zones = width_sp // group
    depth = w_query.shape[0]
    pair = jnp.concatenate([w_key, w_value], axis=1)
    piece = jnp.concatenate(
        [w_query, jnp.concatenate([pair[: depth // 2], pair[depth // 2 :]], axis=1)], axis=0
    )
    q_parts, kv_parts = project(inputs[0], in_gain[None], piece, zones, group, 2 * ck)
    gains = lax.dynamic_slice_in_dim(out_gain, own_index * cq, cq, 0).reshape(1, cq)
    return mixer(q_parts, kv_parts, w_out, key_bias[0].T, gains, zones, group)[None]


def solution(mesh):
    placed = (
        P("dp", "sp", None),
        P(),
        P("dp", "sp"),
        P("dp", "sp"),
        P("dp", "sp"),
        P("dp", None, "sp"),
        P(),
        P("sp", "dp"),
    )
    return jax.shard_map(
        body, mesh=mesh, in_specs=placed, out_specs=P("dp", "sp", None), check_vma=False
    )
```

time: 173 us -> 109 us (0.63)
  the two profiles are of different devices: /device:TPU:0 before, /device:TPU:28 now
where the time goes in v3:
time: 109 us
  Pallas kernels  103 us (94%)
  local copies, waits for them, and re-layouts  5.19 us (5%)
    pallas_call x1, Pallas kernels, mixer(): pl.pallas_call(functools.partial(mixer_kernel, zones, group, block), out_...  66.1 us
    pallas_call x1, Pallas kernels, project(): pl.pallas_call(functools.partial(project_kernel, zones, group), out_shape...  36.7 us
    unnamed x9, local copies, waits for them, and re-layouts  4.59 us

profile of v3, /device:TPU:28, one launch (start us, length us, event | category | flops | bytes accessed | tf_op | source)
XLA Modules:
  0.0 108.9 jit_solution(11706991075479092977)
XLA Ops:
  0.0 0.0 copy-start
  0.0 0.7 copy-done
  0.7 0.6 dynamic-slice_bitcast_fusion.gain_ref
  1.3 0.0 copy-start.2
  1.3 0.9 copy.9
  2.2 0.0 copy-done.2
  2.2 0.1 copy.10
  2.3 0.0 copy-start.1
  2.3 0.1 fusion.8
  2.4 0.8 copy-done.1
  3.2 0.8 fusion.7.piece_ref
  4.0 36.7 %project.1 = (bf16[4,384,128]{2,1,0:T(8,128)(2,1)}, bf16[4,192,128]{2,1,0:T(8,128)(2,1)}) custom-call(bf16[192,2048]{1,0:T(8,128)(2,1)} %bitcast.9, f32[1,2048]{1,0:T(1,128)} %bitcast.11, bf16[768,128]{1,0:T(8,128)(2,1)} %fusion.7.piece_ref), custom_call_target="tpu_custom_call" | custom-call | tf_op jit(solution)/shard_map/project/pallas_call | solution.py:189
  40.8 66.1 %mixer.1 = bf16[192,2048]{1,0:T(8,128)(2,1)} custom-call(bf16[4,384,128]{2,1,0:T(8,128)(2,1)} %get-tuple-element.7.q_ref, bf16[4,192,128]{2,1,0:T(8,128)(2,1)} %get-tuple-element.8.kv_ref, bf16[128,512]{1,0:T(8,128)(2,1)} %w_ref.1, f32[2,1536]{1,0:T(2,128)} %bitcast.10, f32[1,128]{1,0:T(1,128)} %dynamic-slice_bitcast_fusion.gain_ref), custom_call_target="tpu_custom_call" | custom-call | tf_op jit(solution)/shard_map/mixer/pallas_call | solution.py:474
  106.8 2.1 %copy.12 = bf16[1,192,2048]{2,1,0:T(8,128)(2,1)} copy(bf16[1,192,2048]{2,1,0:T(8,128)(2,1)} %bitcast.8) | data formatting | bytes 1572864
Async XLA Ops:
  0.0 0.7 copy-start
  1.3 0.9 copy-start.2
  2.3 0.9 copy-start.1
